TPU v7x, 512 devices: a whole 4x4x16 slice. The times are simulated.
512 devices in a mesh: rep: 2 (over z_hi), fs: 32 (over z_lo, y), tp: 8 (over x, core).
Axes of the slice: x: 4, y: 4, z: 16 (z_hi: 2, z_lo: 8; z = z_hi * 8 + z_lo), core: 2. Of those that a mesh axis runs over, the one named last changes fastest.
Arguments:
- inputs_next: bfloat16 [8192, 2048], P(('rep', 'fs'), 'tp'), parts along dimension 0, may hold values from -6 to 6
- inputs_prev: bfloat16 [8192, 2048], P(('rep', 'fs'), 'tp'), parts along dimension 0, may hold values from -6 to 6
- hidden_prev: bfloat16 [8192, 8192], P(('rep', 'fs')), parts along dimension 0, may hold values from -6 to 6
- cotangent: bfloat16 [8192, 2048], P(('rep', 'fs'), 'tp'), parts along dimension 0, may hold values from -6 to 6
- up_weight: bfloat16 [2048, 8192], P('tp', 'fs'), may hold values from -0.125 to 0.125
- down_weight: bfloat16 [8192, 2048], P('fs', 'tp'), may hold values from -0.0625 to 0.0625
- up_accum: float32 [4096, 8192], P(('rep', 'tp'), 'fs'), parts along dimension 0, may hold values from -192 to 192
- down_accum: float32 [16384, 2048], P(('rep', 'fs'), 'tp'), parts along dimension 0, may hold values from -192 to 192
Outputs:
- output_next: bfloat16 [8192, 2048], P(('rep', 'fs'), 'tp'), parts along dimension 0
- hidden_next: bfloat16 [8192, 8192], P(('rep', 'fs')), parts along dimension 0
- input_grad: bfloat16 [8192, 2048], P(('rep', 'fs'), 'tp'), parts along dimension 0
- up_accum_out: float32 [4096, 8192], P(('rep', 'tp'), 'fs'), parts along dimension 0
- down_accum_out: float32 [16384, 2048], P(('rep', 'fs'), 'tp'), parts along dimension 0
There are 2 independent parts, one for each index of `rep`. A program takes and returns all parts, laid end to end along the dimension named above; an argument that names none is the same for every part. Nothing has to cross between parts.
All inputs are finite; a program needn't handle non-finite values.
Results may differ from a plain program's by a relative error of at most 0.034.
Values may be sent and summed in bfloat16 or wider, within the bound.
A program may use at most 128 MiB of HBM per device.

v0:
```python
import jax
import jax.numpy as jnp
from jax import lax
from jax.sharding import Mesh
from jax.sharding import PartitionSpec as P

FS = ("fs_0", "fs_1")
REP_FS = ("rep", "fs_0", "fs_1")


def joined_along(pieces, dim):
    shape = list(pieces.shape[1:])
    shape[dim] *= pieces.shape[0]
    return jnp.moveaxis(pieces, 0, dim).reshape(shape)


def all_blocks(x, axes, order):
    pieces = x[None]
    for k in order:
        pieces = lax.all_gather(pieces, axes[k], axis=0, tiled=True)
    held = [lax.axis_size(axes[k]) for k in reversed(order)]
    pieces = pieces.reshape(*held, *x.shape)
    turned = sorted(range(len(order)), key=lambda place: order[len(order) - 1 - place])
    return pieces.transpose(*turned, *range(len(order), pieces.ndim)).reshape(-1, *x.shape)


def whole_of(x, axes, order, dim):
    return joined_along(all_blocks(x, axes, order), dim)


def side_by_side(arrays, axis, dim, along):
    ends, at = ([], 0)
    for a in arrays[:-1]:
        at += a.shape[along]
        ends.append(at)
    both = jnp.concatenate(arrays, axis=along)
    return tuple(jnp.split(lax.all_gather(both, axis, axis=dim, tiled=True), ends, axis=along))


def squared_relu(values):
    return jnp.square(jax.nn.relu(values.astype(jnp.float32))).astype(jnp.bfloat16)


def contract(left, right, left_dim, right_dim):
    return lax.dot_general(
        left, right, (((left_dim,), (right_dim,)), ((), ())), preferred_element_type=jnp.float32
    )


def local(
    inputs_next, inputs_prev, hidden_prev, cotangent, up_weight, down_weight, up_accum, down_accum
):
    up_whole = whole_of(up_weight, FS, (0, 1), 1)
    hidden_terms = jnp.dot(inputs_next, up_whole, preferred_element_type=jnp.float32).astype(
        jnp.bfloat16
    )
    hidden_next = lax.psum(hidden_terms, "tp").astype(jnp.float32).astype(jnp.bfloat16)
    acts_next = squared_relu(hidden_next)
    saved_inputs, cotangent_all = side_by_side((inputs_prev, cotangent), FS, 0, 1)
    down_whole = lax.all_gather(down_weight, FS, axis=0, tiled=True)
    output_next = jnp.dot(acts_next, down_whole, preferred_element_type=jnp.float32).astype(
        jnp.bfloat16
    )
    back_terms = contract(cotangent, down_whole, 1, 1).astype(jnp.bfloat16)
    back_sum = lax.psum(back_terms, "tp").astype(jnp.float32)
    hidden_grad = (back_sum * 2.0 * jax.nn.relu(hidden_prev.astype(jnp.float32))).astype(
        jnp.bfloat16
    )
    acts_prev = squared_relu(hidden_prev)
    acts_spread, grad_spread = (
        lax.all_to_all(acts_prev, FS, split_axis=1, concat_axis=0, tiled=True),
        lax.all_to_all(hidden_grad, FS, split_axis=1, concat_axis=0, tiled=True),
    )
    input_grad = contract(hidden_grad, up_whole, 1, 1).astype(jnp.bfloat16)
    up_accum_out = up_accum + contract(saved_inputs, grad_spread, 0, 0)
    down_accum_out = down_accum + contract(acts_spread, cotangent_all, 0, 0)
    return (output_next, hidden_next, input_grad, up_accum_out, down_accum_out)


def solution(mesh):
    finer = Mesh(
        mesh.devices.reshape(mesh.shape["rep"], 8, 4, mesh.shape["tp"]),
        ("rep", "fs_0", "fs_1", "tp"),
    )
    in_specs = (
        P(REP_FS, "tp"),
        P(REP_FS, "tp"),
        P(REP_FS, None),
        P(REP_FS, "tp"),
        P("tp", FS),
        P(FS, "tp"),
        P(("rep", "tp"), FS),
        P(REP_FS, "tp"),
    )
    out_specs = (
        P(REP_FS, "tp"),
        P(REP_FS, None),
        P(REP_FS, "tp"),
        P(("rep", "tp"), FS),
        P(REP_FS, "tp"),
    )
    return jax.shard_map(local, mesh=finer, in_specs=in_specs, out_specs=out_specs, check_vma=False)
```

profile of v0, /device:TPU:134, one launch (start us, length us, event | category | flops | bytes accessed | tf_op | source)
XLA Modules:
  0.0 731.7 jit_solution(9479650889857081731)
XLA Ops:
  7.2 0.0 copy-start
  7.2 0.0 all-gather.12.cloned.1.call-start
  7.2 0.7 all-gather.12.cloned.1.call-update
  7.9 0.0 all-gather.6.cloned.1.call-start
  8.0 60.2 %all-gather.12.cloned.1.call-done = bf16[2048,256]{1,0:T(8,128)(2,1)} async-done(((bf16[256,256]{1,0:T(8,128)(2,1)}), bf16[2048,256]{1,0:T(8,128)(2,1)}) %all-gather.12.cloned.1.call-update) | async-done | bytes 1048592 | tf_op jit(solution)/shard_map/all_gather | solution.py:20
  68.2 0.0 all-gather.6.cloned.1.call-update
  68.2 0.0 all-gather.8.cloned.1.call-start
  68.2 0.7 all-gather.8.cloned.1.call-update
  68.9 0.0 all-reduce.3.cloned.1.call-start
  69.0 63.4 %all-gather.6.cloned.1.call-done = bf16[32,256,256]{2,1,0:T(8,128)(2,1)} async-done(((bf16[8,256,256]{2,1,0:T(8,128)(2,1)}), bf16[32,256,256]{2,1,0:T(8,128)(2,1)}) %all-gather.6.cloned.1.call-update) | async-done | bytes 4194320 | tf_op jit(solution)/shard_map/all_gather | solution.py:20
  132.3 4.6 copy.20
  136.9 6.5 copy.21
  143.4 0.0 copy-start.4
  143.4 0.0 copy-done
  143.4 5.0 convolution_convert_fusion.1
  148.4 162.4 %all-gather.8.cloned.1.call-done = bf16[8192,256]{1,0:T(8,128)(2,1)} async-done(((bf16[256,256]{1,0:T(8,128)(2,1)}), bf16[8192,256]{1,0:T(8,128)(2,1)}) %all-gather.8.cloned.1.call-update) | async-done | bytes 4194320 | tf_op jit(solution)/shard_map/all_gather | solution.py:60
  310.8 0.0 copy-done.4
  310.8 5.0 convolution_convert_fusion
  315.8 0.0 all-reduce.3.cloned.1.call-update
  315.9 134.6 %all-reduce.3.cloned.1.call-done = (bf16[128,8192]{1,0:T(8,128)(2,1)}, bf16[128,8192]{1,0:T(8,128)(2,1)}) async-done(((bf16[128,8192]{1,0:T(8,128)(2,1)}, bf16[128,8192]{1,0:T(8,128)(2,1)}), (bf16[128,8192]{1,0:T(8,128)(2,1)}, bf16[128,8192]{1,0:T(8,128)(2,1)})) %all-reduce.3.cloned.1.call-update) | async-done | bytes 4194320 | tf_op jit(solution)/shard_map/psum | solution.py:57
  450.5 4.6 multiply_convert_fusion
  455.0 0.0 copy-start.5
  455.0 1.6 copy.29
  456.6 12.8 %all-to-all-start = ((bf16[128,32,256]{2,0,1:T(8,128)(2,1)}), bf16[128,32,256]{2,0,1:T(8,128)(2,1)}, u32[]{:S(2)}, u32[]{:S(2)}) async-start(bf16[128,32,256]{2,0,1:T(8,128)(2,1)} %bitcast.36), calls=%async_computation | async-start | bytes 4194304 | tf_op jit(solution)/shard_map/all_to_all | solution.py:72
  469.5 0.0 all-gather.10.cloned.1.call-start
  469.5 0.0 copy-done.5
  469.5 0.7 pad_maximum_fusion
  470.2 0.0 all-gather.10.cloned.1.call-update
  470.2 3.1 copy.28
  473.4 101.6 %all-to-all-done = bf16[128,32,256]{2,0,1:T(8,128)(2,1)} async-done(((bf16[128,32,256]{2,0,1:T(8,128)(2,1)}), bf16[128,32,256]{2,0,1:T(8,128)(2,1)}, u32[]{:S(2)}, u32[]{:S(2)}) %all-to-all-start) | async-done | bytes 2097184 | tf_op jit(solution)/shard_map/all_to_all | solution.py:72
  575.0 16.2 %all-to-all-start.1 = ((bf16[128,32,256]{2,0,1:T(8,128)(2,1)}), bf16[128,32,256]{2,0,1:T(8,128)(2,1)}, u32[]{:S(2)}, u32[]{:S(2)}) async-start(bf16[128,32,256]{2,0,1:T(8,128)(2,1)} %bitcast.35), calls=%async_computation.1 | async-start | bytes 4194304 | tf_op jit(solution)/shard_map/all_to_all | solution.py:71
  591.2 0.0 copy-start.1
  591.2 0.0 copy-start.2
  591.2 3.7 convolution_convert_fusion.2
  594.9 0.0 copy-start.6
  594.9 0.0 copy-done.1
  594.9 0.5 copy-done.2
  595.4 1.3 fusion.12
  596.7 0.0 copy-start.7
  596.7 119.6 %all-gather.10.cloned.1.call-done = bf16[4096,512]{1,0:T(8,128)(2,1)} async-done(((bf16[128,512]{1,0:T(8,128)(2,1)}), bf16[4096,512]{1,0:T(8,128)(2,1)}) %all-gather.10.cloned.1.call-update) | async-done | bytes 4194320 | tf_op jit(solution)/shard_map/all_gather | solution.py:37
  716.3 0.0 copy-done.6
  716.3 3.7 fusion.6
  720.0 0.0 copy-start.3
  720.0 0.0 all-to-all-done.1
  720.0 0.0 copy-done.7
  720.0 3.8 fusion.9
  723.8 0.0 copy-done.3
  723.8 1.3 copy.32
Async XLA Ops:
  7.2 136.2 %copy-start = (bf16[128,256]{1,0:T(8,128)(2,1)S(1)}, bf16[128,256]{1,0:T(8,128)(2,1)}, u32[]{:S(2)}) copy-start(bf16[128,256]{1,0:T(8,128)(2,1)} %param.8) | copy-start | bytes 196612
  7.2 61.0 %all-gather.12.cloned.1.call-start = ((), (), s32[]{:S(2)}) async-start(), calls=%async_computation.5 | async-start | bytes 1179648 | tf_op jit(solution)/shard_map/all_gather | solution.py:20
  7.9 124.4 %all-gather.6.cloned.1.call-start = ((), (), s32[]{:S(2)}) async-start(), calls=%async_computation.2 | async-start | bytes 5242880 | tf_op jit(solution)/shard_map/all_gather | solution.py:20
  68.2 242.7 %all-gather.8.cloned.1.call-start = ((), (), s32[]{:S(2)}) async-start(), calls=%async_computation.3 | async-start | bytes 4325376 | tf_op jit(solution)/shard_map/all_gather | solution.py:60
  68.9 381.6 %all-reduce.3.cloned.1.call-start = ((), (), s32[]{:S(2)}) async-start(), calls=%async_computation.6 | async-start | bytes 8388608 | tf_op jit(solution)/shard_map/psum | solution.py:57
  143.4 167.4 %copy-start.4 = (bf16[128,256]{1,0:T(8,128)(2,1)S(1)}, bf16[128,256]{1,0:T(8,128)(2,1)}, u32[]{:S(2)}) copy-start(bf16[128,256]{1,0:T(8,128)(2,1)} %param.11) | copy-start | bytes 196612
  455.0 14.5 %copy-start.5 = (bf16[128,256]{1,0:T(8,128)(2,1)S(1)}, bf16[128,256]{1,0:T(8,128)(2,1)}, u32[]{:S(2)}) copy-start(bf16[128,256]{1,0:T(8,128)(2,1)} %param.9) | copy-start | bytes 196612
  456.6 118.3 %all-to-all-start = ((bf16[128,32,256]{2,0,1:T(8,128)(2,1)}), bf16[128,32,256]{2,0,1:T(8,128)(2,1)}, u32[]{:S(2)}, u32[]{:S(2)}) async-start(bf16[128,32,256]{2,0,1:T(8,128)(2,1)} %bitcast.36), calls=%async_computation | async-start | bytes 4194304 | tf_op jit(solution)/shard_map/all_to_all | solution.py:72
  469.5 246.8 %all-gather.10.cloned.1.call-start = ((), (), s32[]{:S(2)}) async-start(), calls=%async_computation.4 | async-start | bytes 4325376 | tf_op jit(solution)/shard_map/all_gather | solution.py:37
  575.0 145.0 %all-to-all-start.1 = ((bf16[128,32,256]{2,0,1:T(8,128)(2,1)}), bf16[128,32,256]{2,0,1:T(8,128)(2,1)}, u32[]{:S(2)}, u32[]{:S(2)}) async-start(bf16[128,32,256]{2,0,1:T(8,128)(2,1)} %bitcast.35), calls=%async_computation.1 | async-start | bytes 4194304 | tf_op jit(solution)/shard_map/all_to_all | solution.py:71
  591.2 3.7 copy-start.1
  591.2 4.2 copy-start.2
  594.9 121.4 %copy-start.6 = (f32[256,256]{1,0:T(8,128)S(1)}, f32[256,256]{1,0:T(8,128)}, u32[]{:S(2)}) copy-start(f32[256,256]{1,0:T(8,128)} %param.14) | copy-start | bytes 786436
  596.7 123.3 %copy-start.7 = (f32[256,256]{1,0:T(8,128)S(1)}, f32[256,256]{1,0:T(8,128)}, u32[]{:S(2)}) copy-start(f32[256,256]{1,0:T(8,128)} %param.15) | copy-start | bytes 786436
  720.0 3.8 copy-start.3
Sparse Core Ops, SparseCore 0:
  10.1 58.0 all-gather.11
  70.2 62.0 all-gather.5
  134.4 176.3 all-gather.7
  316.0 134.4 all-reduce.2
  472.6 243.6 all-gather.9
where the time goes:
time: 732 us
  waiting for transfers between devices  643 us (88%)
  starting transfers between devices  29.3 us (4%)
  matrix products  22.5 us (3%)
  local copies, waits for them, and re-layouts  17.6 us (2%)
  between operations  13.8 us (2%)
    all_gather x1, waiting for transfers between devices, local(): down_whole = lax.all_gather(down_weight, FS, axis=0, tiled=True)  162 us
    psum x1, waiting for transfers between devices, local(): lax.psum(hidden_terms, 'tp').astype(jnp.float32).astype(jnp.bfloat16)  135 us
    all_gather x2, waiting for transfers between devices, all_blocks(): pieces = lax.all_gather(pieces, axes[k], axis=0, tiled=True)  124 us
    all_gather x1, waiting for transfers between devices, side_by_side(): lax.all_gather(both, axis, axis=dim, tiled=True)  120 us
    all_to_all x1, waiting for transfers between devices, local(): lax.all_to_all(hidden_grad, FS, split_axis=1, concat_axis=0, tiled=True)  102 us
    all_to_all x1, starting transfers between devices, local(): lax.all_to_all(acts_prev, FS, split_axis=1, concat_axis=0, tiled=True)  16.2 us
    dot_general x4, matrix products, contract(): lax.dot_general(left, right, (((left_dim,), (right_dim,)), ((), ())), pre...  16.2 us
  transfers between devices with their start and end apart: 7, of which 6 were waited for; matrix products, arithmetic and copies ran while one was open for 4% of the time, Pallas kernels for 0%

commit v1 on v0

v1 whole, which is shorter than its diff:
```python
import jax
import jax.numpy as jnp
from jax import lax
from jax.experimental import pallas as pl
from jax.experimental.pallas import tpu as pltpu
from jax.sharding import PartitionSpec as P

BF = jnp.bfloat16
F32 = jnp.float32
MESH = pl.DeviceIdType.MESH

NZ, NY, NX = 8, 4, 4
N_SEMS = 144


def dot(a, b, ca, cb):
    return lax.dot_general(a, b, (((ca,), (cb,)), ((), ())), preferred_element_type=F32)


def relu(v):
    return jnp.maximum(v, 0.0)


class Copies:
    def __init__(self, send, recv):
        self.send, self.recv, self.count, self.always = send, recv, 0, []

    def slot(self):
        self.count += 1
        assert self.count <= N_SEMS
        return self.count - 1

    def at(self, slot, src, dst, to):
        return pltpu.make_async_remote_copy(
            src_ref=src,
            dst_ref=dst,
            send_sem=self.send.at[slot],
            recv_sem=self.recv.at[slot],
            device_id=to,
            device_id_type=MESH,
        )

    def make(self, src, dst, to):
        made = self.at(self.slot(), src, dst, to)
        self.always.append(made)
        return made


class RingGather:
    def __init__(self, copies, me, block, halves, to, own=None):
        up, down = lax.rem(me + 1, 4), lax.rem(me + 3, 4)
        source = block(me) if own is None else own
        self.to_up = copies.make(source, block(me), to(up))
        self.to_down = copies.make(source, block(me), to(down))
        self.on_up = copies.make(halves(down)[0], halves(down)[0], to(up))
        self.on_down = copies.make(halves(up)[1], halves(up)[1], to(down))

    def start(self):
        self.to_up.start()
        self.to_down.start()

    def middle(self):
        self.to_up.wait_recv()
        self.on_up.start()
        self.to_down.wait_recv()
        self.on_down.start()

    def end(self):
        self.on_up.wait_recv()
        self.on_down.wait_recv()


class RingReduce:
    def __init__(self, copies, me, block, halves, to, bufs):
        up, down, far = lax.rem(me + 1, 4), lax.rem(me + 3, 4), lax.rem(me + 2, 4)
        self.half_up, self.half_down, self.full_up, self.full_down = bufs
        self.far_up = copies.make(halves(far)[0], self.half_up, to(up))
        self.far_down = copies.make(halves(far)[1], self.half_down, to(down))
        self.near_up = copies.make(block(up), self.full_up, to(up))
        self.near_down = copies.make(block(down), self.full_down, to(down))
        self.sum_up, self.sum_down, self.mine = halves(up)[0], halves(down)[1], block(me)

    def start(self):
        self.far_up.start()
        self.far_down.start()

    def middle(self):
        self.far_up.wait_recv()
        add_into(self.sum_up, self.half_up)
        self.far_down.wait_recv()
        add_into(self.sum_down, self.half_down)
        self.near_up.start()
        self.near_down.start()

    def end(self):
        self.near_up.wait_recv()
        self.near_down.wait_recv()
        return (
            self.mine[...].astype(F32)
            + self.full_up[...].astype(F32)
            + self.full_down[...].astype(F32)
        )


def add_into(total, term):
    total[...] = (total[...].astype(F32) + term[...].astype(F32)).astype(BF)


def line_order(ready, hop=5.1, each=2.8):
    orders = []
    for plane in range(NZ):
        steps = []
        for way in (0, 1):
            for weight in (0, 1):
                for turn in range(NZ - 1):
                    dest = NZ - 1 - turn if way == 0 else turn
                    far = plane if way == 0 else NZ - 1 - plane
                    if (dest > plane) if way == 0 else (dest < plane):
                        begin = max(ready[1], ready[weight])
                        if weight == 1:
                            begin = ready[1]
                        else:
                            begin = max(ready[0], ready[1] + each * (NZ - 1))
                        at = begin + hop * far + each * turn if far else ready[weight]
                        steps.append((at, turn, way, weight, dest))
        orders.append(sorted(steps))
    return orders


def kernel(
    xn, xp, ct, hp, upw, dnw, upa, dna,
    out, hn_out, ig, ua, da,
    tok, ut, wg, hps, hpf, apt, hpo, hpi, hns, an, hg, hgt, rsb, sa, sb,
    a1u, a1d, a2u, a2d, a3u, a3d, a4u, a4d, b1u, b1d, b2u, b2d, b3u, b3d, b4u, b4d,
    hng, grd, rr, rl, fg, fr, send, recv,
):
    r, f, t = lax.axis_index("rep"), lax.axis_index("fs"), lax.axis_index("tp")
    z, y, x, c = f // NY, lax.rem(f, NY), t // 2, lax.rem(t, 2)
    big_z = r * NZ + z

    def at_x(i):
        return (r, f, i * 2 + c)

    def at_y(j):
        return (r, z * NY + j, t)

    def at_big_z(k):
        return (k // NZ, lax.rem(k, NZ) * NY + y, t)

    partner = (r, f, x * 2 + 1 - c)
    z_up, z_down = at_big_z(lax.rem(big_z + 1, 2 * NZ)), at_big_z(lax.rem(big_z + 2 * NZ - 1, 2 * NZ))
    xs = [lax.rem(x + k, NX) for k in (1, 3, 2)]
    ys = [lax.rem(y + k, NY) for k in (1, 3, 2)]

    barrier = pltpu.get_barrier_semaphore()
    peers = [partner, z_up, z_down] + [at_x(i) for i in xs] + [at_y(j) for j in ys]
    for peer in peers:
        pl.semaphore_signal(barrier, inc=1, device_id=peer, device_id_type=MESH)

    copies = Copies(send, recv)

    up_t = upw[...].astype(F32).T.astype(BF)
    ut[...] = up_t.reshape(4, 64, 256)
    for k, ref in enumerate((xn, ct, xp)):
        tok[k, x, y] = ref[...]
    pl.semaphore_wait(barrier, len(peers))

    spread = []
    for w, source in ((1, dnw), (0, ut)):
        for i in xs:
            spread.append(copies.make(source.at[i], wg.at[w, x, z], at_x(i)))
    for s in spread:
        s.start()
    wg[1, x, z] = dnw[x]
    wg[0, x, z] = ut[x]

    first_a, first_b, second_a, second_b = {}, {}, {}, {}
    for k, ref in ((1, ct), (0, xn), (2, xp)):
        first_a[k] = RingGather(
            copies, x,
            lambda i, k=k: tok.at[k, i, y, 0:64],
            lambda i, k=k: (tok.at[k, i, y, 0:32], tok.at[k, i, y, 32:64]),
            at_x, ref.at[0:64],
        )
        first_b[k] = RingGather(
            copies, y,
            lambda j, k=k: tok.at[k, x, j, 64:128],
            lambda j, k=k: (tok.at[k, x, j, 64:96], tok.at[k, x, j, 96:128]),
            at_y, ref.at[64:128],
        )
        second_a[k] = RingGather(
            copies, y,
            lambda j, k=k: tok.at[k, :, j, 0:64],
            lambda j, k=k: (tok.at[k, 0:2, j, 0:64], tok.at[k, 2:4, j, 0:64]),
            at_y,
        )
        second_b[k] = RingGather(
            copies, x,
            lambda i, k=k: tok.at[k, i, :, 64:128],
            lambda i, k=k: (tok.at[k, i, 0:2, 64:128], tok.at[k, i, 2:4, 64:128]),
            at_x,
        )
    for k in (1, 0, 2):
        first_a[k].start()
        first_b[k].start()

    lane = lax.broadcasted_iota(jnp.int32, (128, 128), 1)
    low = lane < 64
    odd = lax.rem(x, 2) == 1
    for j in range(NY):
        for m in range(2):
            off = 1024 * (4 * c + 2 * m) + 256 * j + 128 * (x // 2)
            one = hp[:, pl.ds(pl.multiple_of(off, 128), 128)].astype(F32)
            two = hp[:, pl.ds(pl.multiple_of(off + 1024, 128), 128)].astype(F32)
            left = jnp.where(odd, pltpu.roll(one, 64, axis=1), one)
            right = jnp.where(odd, two, pltpu.roll(two, 64, axis=1))
            hps[j, :, 128 * m:128 * m + 128] = jnp.where(low, left, right).astype(BF)
    hpf[c, y] = hps[y]

    for s in spread:
        s.wait_recv()
    gather_z = {}
    for w, rights, lefts in ((1, 3, 4), (0, 4, 3)):
        for way, steps, to in ((0, rights, z_up), (1, lefts, z_down)):
            made = []
            for s in range(steps):
                piece = lax.rem(z + (NZ - s if way == 0 else s), NZ)
                made.append(copies.make(wg.at[w, :, piece], wg.at[w, :, piece], to))
            gather_z[w, way] = made

    def step_z(s):
        for w in (1, 0):
            for way in (0, 1):
                made = gather_z[w, way]
                if 1 <= s <= len(made):
                    made[s - 1].wait_recv()
                if s < len(made):
                    made[s].start()

    step_z(0)
    hp_sends = [copies.make(hps.at[j], hpf.at[c, y], at_y(j)) for j in ys]
    for s in hp_sends:
        s.start()

    for k in (1, 0, 2):
        first_a[k].middle()
        first_b[k].middle()
    for k in (1, 0, 2):
        first_a[k].end()
        first_b[k].end()
        second_a[k].start()
        second_b[k].start()
    for s in hp_sends:
        s.wait_recv()
    hp_pair = copies.make(hpf.at[c], hpf.at[c], partner)
    hp_pair.start()
    step_z(1)
    second_a[1].middle()
    second_b[1].middle()
    second_a[0].middle()
    second_b[0].middle()

    hp_pair.wait_recv()
    for h in range(2):
        for j in range(NY):
            v = relu(hpf[h, j].astype(F32))
            apt[256 * h:256 * h + 256, 128 * j:128 * j + 128] = (
                (v * v).astype(BF).astype(F32).T.astype(BF)
            )
    step_z(2)
    second_a[1].end()
    second_b[1].end()
    second_a[2].middle()
    second_b[2].middle()

    def partial_gradient(w, left, k):
        def body(i, carry):
            right = tok[k, i].reshape(512, 256)
            for h in range(2):
                got = dot(left[256 * h:256 * h + 256, :], right, 1, 0).astype(BF)
                grd[w, i, 4 * h:4 * h + 4] = got.reshape(4, 64, 256)
            return carry

        lax.fori_loop(0, NX, body, 0)

    partial_gradient(1, apt, 1)
    step_z(3)

    base_line = {}
    for way in (0, 1):
        for w in (0, 1):
            base_line[way, w] = [copies.slot() for _ in range(NZ)]
    line_bufs = (rr, rl)

    def line_copy(plane, way, w, dest):
        buf = line_bufs[way]
        first = plane == (0 if way == 0 else NZ - 1)
        source = grd.at[w, :, dest] if first else buf.at[w, dest]
        to = (r, f + NY if way == 0 else f - NY, t)
        return copies.at(base_line[way, w][dest], source, buf.at[w, dest], to), first

    def line_step(plane, way, w, dest):
        made, first = line_copy(plane, way, w, dest)
        if not first:
            made.wait_recv()
            buf = line_bufs[way]

            def body(i, carry):
                buf[w, dest, i] = (
                    buf[w, dest, i].astype(F32) + grd[w, i, dest].astype(F32)
                ).astype(BF)
                return carry

            lax.fori_loop(0, NX, body, 0)
        made.start()

    orders = line_order((34.0, 22.0))
    done = [0] * NZ

    def line_until(time, weights=(0, 1)):
        for plane in range(NZ):
            todo = []
            while done[plane] < len(orders[plane]) and orders[plane][done[plane]][0] <= time:
                todo.append(orders[plane][done[plane]])
                done[plane] += 1
            if todo:

                @pl.when(z == plane)
                def _():
                    for _, _, way, w, dest in todo:
                        line_step(plane, way, w, dest)

    line_until(24.0)
    second_a[0].end()
    second_b[0].end()
    step_z(4)

    def partial_hidden(q, w):
        def body(j, carry):
            for h in range(2):
                total = None
                for i in range(NX):
                    part = dot(
                        tok[q, i, pl.ds(2 * j, 2)].reshape(256, 256),
                        wg[w, i, 4 * h:4 * h + 4].reshape(256, 256),
                        1, 1,
                    )
                    total = part if total is None else total + part
                hpo[q, h, pl.ds(2 * j, 2)] = total.astype(BF).reshape(2, 128, 256)
            return carry

        lax.fori_loop(0, 2, body, 0)

    pair = [copies.make(hpo.at[q], hpi.at[q], partner) for q in range(2)]
    partial_hidden(1, 1)
    pair[1].start()
    partial_hidden(0, 0)
    pair[0].start()
    pair[1].wait_recv()
    for h in range(2):
        for j in range(NY):
            back = hpo[1, h, j].astype(F32) + hpi[1, h, j].astype(F32)
            grad = (back * 2.0 * relu(hpf[h, j].astype(F32))).astype(BF)
            hg[h, j] = grad
            hgt[256 * h:256 * h + 256, 128 * j:128 * j + 128] = grad.astype(F32).T.astype(BF)
    pair[0].wait_recv()
    for h in range(2):
        for j in range(NY):
            hidden = (hpo[0, h, j].astype(F32) + hpi[0, h, j].astype(F32)).astype(BF)
            hns[h, j] = hidden
            v = relu(hidden.astype(F32))
            an[h, j] = (v * v).astype(BF)

    second_a[2].end()
    second_b[2].end()
    partial_gradient(0, hgt, 2)
    line_until(34.0)

    hn_sends = [copies.make(hns.at[c, j], hng.at[c, x, y], at_y(j)) for j in ys]
    for s in hn_sends:
        s.start()
    hng[c, x, y] = hns[c, y]

    def partial_output(q, left, w):
        def body(i, carry):
            for j in range(2):
                total = None
                for h in range(2):
                    part = dot(
                        left[h, 2 * j:2 * j + 2].reshape(256, 256),
                        wg[w, i, 4 * h:4 * h + 4].reshape(256, 256),
                        1, 0,
                    )
                    total = part if total is None else total + part
                rsb[q, i, 2 * j:2 * j + 2] = total.astype(BF).reshape(2, 128, 256)
            return carry

        lax.fori_loop(0, NX, body, 0)

    partial_output(0, an, 1)
    partial_output(1, hg, 0)

    reduce_a1 = RingReduce(
        copies, x,
        lambda i: rsb.at[:, i, :, 0:64],
        lambda i: (rsb.at[:, i, 0:2, 0:64], rsb.at[:, i, 2:4, 0:64]),
        at_x, (a1u, a1d, a2u, a2d),
    )
    reduce_b1 = RingReduce(
        copies, y,
        lambda j: rsb.at[:, :, j, 64:128],
        lambda j: (rsb.at[:, 0:2, j, 64:128], rsb.at[:, 2:4, j, 64:128]),
        at_y, (b1u, b1d, b2u, b2d),
    )
    reduce_a2 = RingReduce(
        copies, y,
        lambda j: sa.at[:, j],
        lambda j: (sa.at[:, j, 0:32], sa.at[:, j, 32:64]),
        at_y, (a3u, a3d, a4u, a4d),
    )
    reduce_b2 = RingReduce(
        copies, x,
        lambda i: sb.at[:, i],
        lambda i: (sb.at[:, i, 0:32], sb.at[:, i, 32:64]),
        at_x, (b3u, b3d, b4u, b4d),
    )
    hn_ring = RingGather(
        copies, x, lambda i: hng.at[c, i], lambda i: (hng.at[c, i, 0:2], hng.at[c, i, 2:4]), at_x
    )
    hn_pair = [copies.make(hng.at[c, i], hng.at[c, i], partner) for i in [x] + xs]

    reduce_a1.start()
    reduce_b1.start()
    line_until(38.0)
    for s in hn_sends:
        s.wait_recv()
    hn_ring.start()
    hn_pair[0].start()
    line_until(41.0)
    reduce_a1.middle()
    reduce_b1.middle()
    line_until(45.0)
    hn_ring.middle()
    hn_pair[1].start()
    hn_pair[2].start()
    line_until(50.0)
    sa[...] = reduce_a1.end().astype(BF)
    sb[...] = reduce_b1.end().astype(BF)
    reduce_a2.start()
    reduce_b2.start()
    line_until(53.0)
    hn_ring.end()
    hn_pair[3].start()
    reduce_a2.middle()
    reduce_b2.middle()
    line_until(57.0)
    total = reduce_a2.end()
    out[0:64, :] = total[0].astype(BF)
    ig[0:64, :] = total[1].astype(BF)
    total = reduce_b2.end()
    out[64:128, :] = total[0].astype(BF)
    ig[64:128, :] = total[1].astype(BF)
    for s in hn_pair:
        s.wait_recv()
    for h in range(2):
        for n in range(2):
            for m in range(2):
                for j in range(NY):
                    one = hng[h, 2 * m, j, :, 128 * n:128 * n + 128].astype(F32)
                    two = hng[h, 2 * m + 1, j, :, 128 * n:128 * n + 128].astype(F32)
                    off = 1024 * (4 * h + 2 * n) + 256 * j + 128 * m
                    hn_out[:, off:off + 128] = jnp.where(
                        low, one, pltpu.roll(two, 64, axis=1)
                    ).astype(BF)
                    hn_out[:, off + 1024:off + 1152] = jnp.where(
                        low, pltpu.roll(one, 64, axis=1), two
                    ).astype(BF)

    line_until(1e9)
    for plane in range(NZ):

        @pl.when(z == plane)
        def _():
            for w in (0, 1):
                if plane > 0:
                    line_copy(plane, 0, w, plane)[0].wait_recv()
                else:
                    rr[w, 0] = jnp.zeros((4, 64, 256), BF)
                if plane < NZ - 1:
                    line_copy(plane, 1, w, plane)[0].wait_recv()
                else:
                    rl[w, NZ - 1] = jnp.zeros((4, 64, 256), BF)

    for w in (0, 1):
        fg[w] = (
            grd[w, :, z].astype(F32) + rr[w, z].astype(F32) + rl[w, z].astype(F32)
        ).astype(BF)
    final = [copies.make(fg.at[w, i], fr.at[w, x], at_x(i)) for w in (0, 1) for i in xs]
    for s in final:
        s.start()
    for w in (0, 1):
        fr[w, x] = fg[w, x]
    for s in final:
        s.wait_recv()
    ua[...] = upa[...] + fr[0].reshape(256, 256).astype(F32).T
    da[...] = dna[...] + fr[1].reshape(256, 256).astype(F32)

    for made in copies.always:
        made.wait_send()
    for plane in range(NZ):

        @pl.when(z == plane)
        def _():
            for _, _, way, w, dest in orders[plane]:
                line_copy(plane, way, w, dest)[0].wait_send()


def local(inputs_next, inputs_prev, hidden_prev, cotangent, up_weight, down_weight, up_accum, down_accum):
    vmem = pl.BlockSpec(memory_space=pltpu.VMEM)
    shapes = [
        (3, 4, 4, 128, 256),
        (4, 64, 256),
        (2, 4, 8, 64, 256),
        (4, 128, 256),
        (2, 4, 128, 256),
        (512, 512),
        (2, 2, 4, 128, 256),
        (2, 2, 4, 128, 256),
        (2, 4, 128, 256),
        (2, 4, 128, 256),
        (2, 4, 128, 256),
        (512, 512),
        (2, 4, 4, 128, 256),
        (2, 4, 64, 256),
        (2, 4, 64, 256),
    ]
    for _ in range(2):
        shapes += [(2, 2, 64, 256)] * 2 + [(2, 4, 64, 256)] * 2
        shapes += [(2, 32, 256)] * 2 + [(2, 64, 256)] * 2
    shapes += [
        (2, 4, 4, 128, 256),
        (2, 4, 8, 64, 256),
        (2, 8, 4, 64, 256),
        (2, 8, 4, 64, 256),
        (2, 4, 64, 256),
        (2, 4, 64, 256),
    ]
    outs = [
        (inputs_next.shape, BF),
        (hidden_prev.shape, BF),
        (inputs_prev.shape, BF),
        (up_accum.shape, F32),
        (down_accum.shape, F32),
    ]
    return pl.pallas_call(
        kernel,
        out_shape=tuple(jax.ShapeDtypeStruct(s, d) for s, d in outs),
        in_specs=[vmem] * 8,
        out_specs=(vmem,) * 5,
        scratch_shapes=[pltpu.VMEM(s, BF) for s in shapes]
        + [pltpu.SemaphoreType.DMA((N_SEMS,)), pltpu.SemaphoreType.DMA((N_SEMS,))],
        compiler_params=pltpu.CompilerParams(
            collective_id=0, has_side_effects=True, vmem_limit_bytes=60 * 1024 * 1024
        ),
    )(
        inputs_next, inputs_prev, cotangent, hidden_prev, up_weight,
        down_weight.reshape(4, 64, 256), up_accum, down_accum,
    )


def solution(mesh):
    rep_fs, fs = ("rep", "fs"), "fs"
    in_specs = (
        P(rep_fs, "tp"),
        P(rep_fs, "tp"),
        P(rep_fs, None),
        P(rep_fs, "tp"),
        P("tp", fs),
        P(fs, "tp"),
        P(("rep", "tp"), fs),
        P(rep_fs, "tp"),
    )
    out_specs = (
        P(rep_fs, "tp"),
        P(rep_fs, None),
        P(rep_fs, "tp"),
        P(("rep", "tp"), fs),
        P(rep_fs, "tp"),
    )
    return jax.shard_map(local, mesh=mesh, in_specs=in_specs, out_specs=out_specs, check_vma=False)
```

time: 732 us -> 114 us (0.16)
  the two profiles are of different devices: /device:TPU:134 before, /device:TPU:1 now
where the time goes in v1:
time: 114 us; the launch traced here: 112 us
  Pallas kernels  105 us (92%)
  local copies, waits for them, and re-layouts  6.68 us (6%)
    pallas_call x1, Pallas kernels, local(): pl.pallas_call(kernel, out_shape=tuple((jax.ShapeDtypeStruct(s, d) for s,...  105 us
    unnamed x11, local copies, waits for them, and re-layouts  6.68 us

profile of v1, /device:TPU:1, one launch (start us, length us, event | category | flops | bytes accessed | tf_op | source)
XLA Modules:
  0.0 112.4 jit_solution(990810861156327283)
XLA Ops:
  0.6 105.0 %shard_map.119 = (bf16[128,256]{1,0:T(8,128)(2,1)}, bf16[128,8192]{1,0:T(8,128)(2,1)}, bf16[128,256]{1,0:T(8,128)(2,1)}, f32[256,256]{1,0:T(8,128)}, f32[256,256]{1,0:T(8,128)}) custom-call(bf16[128,256]{1,0:T(8,128)(2,1)} %xn.1, bf16[128,256]{1,0:T(8,128)(2,1)} %xp.1, bf16[128,256]{1,0:T(8,128)(2,1)} %ct.1, bf16[128,8192]{1,0:T(8,128)(2,1)} %hp.1, ...), custom_call_target="tpu_custom_call" | custom-call | tf_op jit(solution)/shard_map/pallas_call | solution.py:555
  105.7 1.5 %copy.18 = bf16[128,256]{1,0:T(8,128)(2,1)} copy(bf16[128,256]{1,0:T(8,128)(2,1)} %get-tuple-element.10) | data formatting | bytes 131072
  107.2 0.0 copy-start.2
  107.2 0.0 copy-start.1
  107.2 0.0 copy-start
  107.2 3.2 %copy.19 = bf16[128,8192]{1,0:T(8,128)(2,1)} copy(bf16[128,8192]{1,0:T(8,128)(2,1)} %get-tuple-element.11) | data formatting | bytes 4194304
  110.3 0.0 copy-done.2
  110.3 0.6 copy.20
  111.0 0.0 copy-done.1
  111.0 0.7 copy.21
  111.7 0.0 copy-done
  111.7 0.7 copy.22
Async XLA Ops:
  107.2 3.2 %copy-start.2 = (bf16[128,256]{1,0:T(8,128)(2,1)S(1)}, bf16[128,256]{1,0:T(8,128)(2,1)}, u32[]{:S(2)}) copy-start(bf16[128,256]{1,0:T(8,128)(2,1)} %get-tuple-element.12) | copy-start | bytes 196612
  107.2 3.8 %copy-start.1 = (f32[256,256]{1,0:T(8,128)S(1)}, f32[256,256]{1,0:T(8,128)}, u32[]{:S(2)}) copy-start(f32[256,256]{1,0:T(8,128)} %get-tuple-element.13) | copy-start | bytes 786436
  107.2 4.5 %copy-start = (f32[256,256]{1,0:T(8,128)S(1)}, f32[256,256]{1,0:T(8,128)}, u32[]{:S(2)}) copy-start(f32[256,256]{1,0:T(8,128)} %get-tuple-element.14) | copy-start | bytes 786436

commit v2 on v1

v2 whole, which is shorter than its diff:
```python
import jax
import jax.numpy as jnp
from jax import lax
from jax.experimental import pallas as pl
from jax.experimental.pallas import tpu as pltpu
from jax.sharding import PartitionSpec as P

BF = jnp.bfloat16
F32 = jnp.float32
MESH = pl.DeviceIdType.MESH

NZ, NY, NX = 8, 4, 4
PARTS = 2
VMEM_MAIN = 60 * 1024 * 1024
W0_READY, W1_READY, EARLY = 35.05, 19.5, 5
LATE = (41.0, 44.5, 51.0, 57.0, 60.0, 62.0, 66.0)
N_SEMS = 256


def dot(a, b, ca, cb):
    return lax.dot_general(a, b, (((ca,), (cb,)), ((), ())), preferred_element_type=F32)


def relu(v):
    return jnp.maximum(v, 0.0)


class Copies:
    def __init__(self, send, recv):
        self.send, self.recv, self.count, self.always = send, recv, 0, []

    def slot(self):
        self.count += 1
        assert self.count <= N_SEMS
        return self.count - 1

    def at(self, slot, src, dst, to):
        return pltpu.make_async_remote_copy(
            src_ref=src,
            dst_ref=dst,
            send_sem=self.send.at[slot],
            recv_sem=self.recv.at[slot],
            device_id=to,
            device_id_type=MESH,
        )

    def make(self, src, dst, to):
        made = self.at(self.slot(), src, dst, to)
        self.always.append(made)
        return made


class RingGather:
    def __init__(self, copies, me, block, halves, to):
        up, down = lax.rem(me + 1, 4), lax.rem(me + 3, 4)
        self.to_up = copies.make(block(me), block(me), to(up))
        self.to_down = copies.make(block(me), block(me), to(down))
        self.on_up = copies.make(halves(down)[0], halves(down)[0], to(up))
        self.on_down = copies.make(halves(up)[1], halves(up)[1], to(down))

    def start(self):
        self.to_up.start()
        self.to_down.start()

    def middle(self):
        self.to_up.wait_recv()
        self.on_up.start()
        self.to_down.wait_recv()
        self.on_down.start()

    def end(self):
        self.on_up.wait_recv()
        self.on_down.wait_recv()


class RingReduce:
    def __init__(self, copies, me, block, halves, to, bufs):
        up, down, far = lax.rem(me + 1, 4), lax.rem(me + 3, 4), lax.rem(me + 2, 4)
        self.half_up, self.half_down, self.full_up, self.full_down = bufs
        self.far_up = copies.make(halves(far)[0], self.half_up, to(up))
        self.far_down = copies.make(halves(far)[1], self.half_down, to(down))
        self.near_up = copies.make(block(up), self.full_up, to(up))
        self.near_down = copies.make(block(down), self.full_down, to(down))
        self.sum_up, self.sum_down, self.mine = halves(up)[0], halves(down)[1], block(me)

    def start(self):
        self.far_up.start()
        self.far_down.start()

    def middle(self):
        self.far_up.wait_recv()
        add_into(self.sum_up, self.half_up)
        self.far_down.wait_recv()
        add_into(self.sum_down, self.half_down)
        self.near_up.start()
        self.near_down.start()

    def end(self):
        self.near_up.wait_recv()
        self.near_down.wait_recv()
        return (
            self.mine[...].astype(F32)
            + self.full_up[...].astype(F32)
            + self.full_down[...].astype(F32)
        )


def add_into(total, term):
    total[...] = (total[...].astype(F32) + term[...].astype(F32)).astype(BF)


def line_order(ready, early):
    orders = [[] for _ in range(NZ)]
    for way in (0, 1):
        free = [5.0 + 5.6 * n for n in (3, 3, 3, 4, 4, 4, 4)]
        queue = []
        for turn in range(NZ - 1):
            for part in range(PARTS):
                queue.append((ready[1], 1, turn, part) if turn < early else (ready[0] + 0.01, 1, turn, part))
                queue.append((ready[0], 0, turn, part))
        queue.sort()
        for at, weight, turn, part in queue:
            for hop in range(NZ - 1 - turn):
                plane = hop if way == 0 else NZ - 1 - hop
                dest = NZ - 1 - turn if way == 0 else turn
                begin = max(free[hop], at)
                orders[plane].append((max(at, begin - 0.7) if hop == 0 else at, way, weight, dest, part))
                free[hop] = begin + 2.8 / PARTS
                at = begin + 2.8 / PARTS + 2.5
    return [sorted(o) for o in orders]


def kernel(
    xn_hbm, xp_hbm, ct_hbm, hp_hbm, up_hbm, dn_hbm,
    out, ig, hng, fr,
    hp, upw, dnw, tok, ut, wg, hps, hpf, apt, hpo, hpi, hns, an, hg, hgt, rsb, sa, sb,
    a1u, a1d, a2u, a2d, a3u, a3d, a4u, a4d, b1u, b1d, b2u, b2d, b3u, b3d, b4u, b4d,
    grd, rr, rl, fg, load, send, recv,
):
    r, f, t = lax.axis_index("rep"), lax.axis_index("fs"), lax.axis_index("tp")
    z, y, x, c = f // NY, lax.rem(f, NY), t // 2, lax.rem(t, 2)
    big_z = r * NZ + z

    def at_x(i):
        return (r, f, i * 2 + c)

    def at_y(j):
        return (r, z * NY + j, t)

    def at_big_z(k):
        return (k // NZ, lax.rem(k, NZ) * NY + y, t)

    partner = (r, f, x * 2 + 1 - c)
    z_up, z_down = at_big_z(lax.rem(big_z + 1, 2 * NZ)), at_big_z(lax.rem(big_z + 2 * NZ - 1, 2 * NZ))
    xs = [lax.rem(x + k, NX) for k in (1, 3, 2)]
    ys = [lax.rem(y + k, NY) for k in (1, 3, 2)]

    loads = [
        pltpu.make_async_copy(source, target, load.at[k])
        for k, (source, target) in enumerate((
            (up_hbm, upw), (dn_hbm, dnw), (dn_hbm.at[x], wg.at[1, x, z]),
            (ct_hbm, tok.at[1, x, y]), (xn_hbm, tok.at[0, x, y]), (xp_hbm, tok.at[2, x, y]), (hp_hbm, hp),
        ))
    ]
    for made in loads:
        made.start()
    barrier = pltpu.get_barrier_semaphore()
    peers = [partner, z_up, z_down] + [at_x(i) for i in xs] + [at_y(j) for j in ys]
    for peer in peers:
        pl.semaphore_signal(barrier, inc=1, device_id=peer, device_id_type=MESH)

    copies = Copies(send, recv)

    for made in loads[:3]:
        made.wait()
    ut[...] = upw[...].astype(F32).T.astype(BF).reshape(4, 64, 256)
    wg[0, x, z] = ut[x]
    pl.semaphore_wait(barrier, len(peers))

    steps = []

    def at(time, name, act):
        steps.append((time, len(steps), name, act))

    spread = {}
    for off, i in ((1, xs[0]), (3, xs[1]), (2, xs[2])):
        for w, source in ((1, dnw), (0, ut)):
            spread[w, off] = copies.make(source.at[i], wg.at[w, x, z], at_x(i))
    for off in (1, 3):
        for w in (1, 0):
            spread[w, off].start()
    at(4.65, "spread2", lambda: [spread[w, 2].start() for w in (1, 0)])
    slabs = (x, xs[0], xs[1], xs[2])
    gather_z = {}
    for w in (1, 0):
        for way, to in ((0, z_up), (1, z_down)):
            for s in range(4):
                piece = lax.rem(z + (NZ - s if way == 0 else s), NZ)
                for k, i in enumerate(slabs):
                    slot = copies.slot()
                    gather_z[w, way, s, k] = copies.at(slot, wg.at[w, i, piece], wg.at[w, i, piece], to)

    sends_far = (jnp.logical_and(z >= 3, z <= 6), jnp.logical_and(z >= 1, z <= 4))
    takes_far = (z >= 4, z < 4)

    def step_z(s, k):
        if s == 0:
            if k:
                for w in (1, 0):
                    spread[w, (0, 3, 1, 2)[k]].wait_recv()
            for w in (1, 0):
                for way in (0, 1):
                    gather_z[w, way, 0, k].start()
            return
        for way in (0, 1):
            if s <= 3:
                for w in (1, 0):
                    gather_z[w, way, s - 1, k].wait_recv()
                    if s < 3:
                        gather_z[w, way, s, k].start()
                if s == 3:

                    @pl.when(sends_far[way])
                    def _():
                        for w in (1, 0):
                            gather_z[w, way, 3, k].start()

            else:

                @pl.when(takes_far[way])
                def _():
                    for w in (1, 0):
                        gather_z[w, way, 3, k].wait_recv()

    z_times = (
        (3.2, 6.5, 6.6, 9.9), (7.15, 10.5, 11.1, 13.3), (13.7, 15.1, 16.5, 18.0),
        (19.5, 21.1, 22.5, 24.1), (25.1, 26.5, 28.0, 29.5),
    )
    for s, row in enumerate(z_times):
        for k, time in enumerate(row):
            at(time, f"z{s}{k}", lambda s=s, k=k: step_z(s, k))

    for made in loads[3:6]:
        made.wait()
    token_times = {
        1: ((4.6, 7.25, 10.35), (10.4, 14.95, 18.2), (3.25, 5.8, 8.0), (8.5, 13.2, 16.4)),
        0: ((11.3, 13.9, 16.75), (16.8, 21.4, 24.6), (3.9, 6.45, 8.7), (15.0, 19.6, 22.8)),
        2: ((12.0, 14.6, 17.1), (19.65, 24.5, 27.9), (4.7, 7.2, 9.4), (17.7, 23.1, 26.3)),
    }
    for k, times in token_times.items():
        first = (
            RingGather(
                copies, x,
                lambda i, k=k: tok.at[k, i, y, 0:64],
                lambda i, k=k: (tok.at[k, i, y, 0:32], tok.at[k, i, y, 32:64]),
                at_x,
            ),
            RingGather(
                copies, y,
                lambda j, k=k: tok.at[k, x, j, 64:128],
                lambda j, k=k: (tok.at[k, x, j, 64:96], tok.at[k, x, j, 96:128]),
                at_y,
            ),
        )
        second = (
            RingGather(
                copies, y,
                lambda j, k=k: tok.at[k, :, j, 0:64],
                lambda j, k=k: (tok.at[k, 0:2, j, 0:64], tok.at[k, 2:4, j, 0:64]),
                at_y,
            ),
            RingGather(
                copies, x,
                lambda i, k=k: tok.at[k, i, :, 64:128],
                lambda i, k=k: (tok.at[k, i, 0:2, 64:128], tok.at[k, i, 2:4, 64:128]),
                at_x,
            ),
        )

        for ring, moments, label in zip((first[0], second[0], first[1], second[1]), times, "abcd"):
            for moment, name in zip(moments, ("start", "middle", "end")):
                at(moment, f"t{k}{label}{name}", getattr(ring, name))

    hp_sends = [copies.make(hps.at[j], hpf.at[c, y], at_y(j)) for j in ys]
    hp_pair = copies.make(hpf.at[c], hpf.at[c], partner)

    def hp_first():
        loads[6].wait()
        low = lax.broadcasted_iota(jnp.int32, (128, 128), 1) < 64
        odd = lax.rem(x, 2) == 1
        for j in range(NY):
            for m in range(2):
                off = 1024 * (4 * c + 2 * m) + 256 * j + 128 * (x // 2)
                one = hp[:, pl.ds(pl.multiple_of(off, 128), 128)].astype(F32)
                two = hp[:, pl.ds(pl.multiple_of(off + 1024, 128), 128)].astype(F32)
                left = jnp.where(odd, pltpu.roll(one, 64, axis=1), one)
                right = jnp.where(odd, two, pltpu.roll(two, 64, axis=1))
                hps[j, :, 128 * m:128 * m + 128] = jnp.where(low, left, right).astype(BF)
        hpf[c, y] = hps[y]

    def start_all(made):
        return lambda: [m.start() for m in made]

    def hp_second():
        for m in hp_sends:
            m.wait_recv()
        hp_pair.start()

    def transpose_acts():
        hp_pair.wait_recv()
        for h in range(2):
            for j in range(NY):
                v = relu(hpf[h, j].astype(F32))
                apt[256 * h:256 * h + 256, 128 * j:128 * j + 128] = (v * v).astype(BF).astype(F32).T.astype(BF)

    at(3.4, "hp_first", hp_first)
    at(7.5, "hp_send", start_all(hp_sends))
    at(13.0, "hp_second", hp_second)
    at(14.7, "acts_prev", transpose_acts)

    def partial_gradient(w, left, k):
        def body(i, carry):
            right = tok[k, i].reshape(512, 256)
            for h in range(2):
                got = dot(left[256 * h:256 * h + 256, :], right, 1, 0).astype(BF)
                grd[w, i, 4 * h:4 * h + 4] = got.reshape(4, 64, 256)
            return carry

        lax.fori_loop(0, NX, body, 0)

    at(18.25, "grad1", lambda: partial_gradient(1, apt, 1))

    line_slots = {
        (way, w, part): [copies.slot() for _ in range(NZ)]
        for way in (0, 1) for w in (0, 1) for part in range(PARTS)
    }
    line_bufs = (rr, rl)
    size = NX // PARTS

    def line_copy(plane, way, w, dest, part):
        buf = line_bufs[way]
        first = plane == (0 if way == 0 else NZ - 1)
        span = pl.ds(part * size, size)
        source = grd.at[w, span, dest] if first else buf.at[w, dest, span]
        to = (r, f + NY if way == 0 else f - NY, t)
        return copies.at(line_slots[way, w, part][dest], source, buf.at[w, dest, span], to), first

    def line_step(plane, way, w, dest, part):
        made, first = line_copy(plane, way, w, dest, part)
        if not first:
            made.wait_recv()
            buf = line_bufs[way]
            for i in range(part * size, part * size + size):
                add_into(buf.at[w, dest, i], grd.at[w, i, dest])
        made.start()

    orders = line_order((W0_READY, W1_READY), EARLY)
    done = [0] * NZ

    def line_until(time):
        for plane in range(NZ):
            todo = []
            while done[plane] < len(orders[plane]) and orders[plane][done[plane]][0] <= time:
                todo.append(orders[plane][done[plane]])
                done[plane] += 1
            if todo:

                @pl.when(z == plane)
                def _():
                    for _, *step in todo:
                        line_step(plane, *step)

    def partial_hidden(q, w):
        def body(j, carry):
            for h in range(2):
                total = None
                for i in range(NX):
                    part = dot(
                        tok[q, i, pl.ds(2 * j, 2)].reshape(256, 256),
                        wg[w, i, 4 * h:4 * h + 4].reshape(256, 256),
                        1, 1,
                    )
                    total = part if total is None else total + part
                hpo[q, h, pl.ds(2 * j, 2)] = total.astype(BF).reshape(2, 128, 256)
            return carry

        lax.fori_loop(0, 2, body, 0)

    pair = [copies.make(hpo.at[q], hpi.at[q], partner) for q in range(2)]

    def hidden_sums():
        partial_hidden(1, 1)
        pair[1].start()
        partial_hidden(0, 0)
        pair[0].start()

    def hidden_gradient():
        pair[1].wait_recv()
        for h in range(2):
            for j in range(NY):
                back = hpo[1, h, j].astype(F32) + hpi[1, h, j].astype(F32)
                grad = (back * 2.0 * relu(hpf[h, j].astype(F32))).astype(BF)
                hg[h, j] = grad
                hgt[256 * h:256 * h + 256, 128 * j:128 * j + 128] = grad.astype(F32).T.astype(BF)

    def hidden_acts():
        pair[0].wait_recv()
        for h in range(2):
            for j in range(NY):
                hidden = (hpo[0, h, j].astype(F32) + hpi[0, h, j].astype(F32)).astype(BF)
                hns[h, j] = hidden
                v = relu(hidden.astype(F32))
                an[h, j] = (v * v).astype(BF)

    hn_sends = [copies.make(hns.at[c, j], hng.at[c, x, y], at_y(j)) for j in ys]
    hn_ring = RingGather(
        copies, x, lambda i: hng.at[c, i], lambda i: (hng.at[c, i, 0:2], hng.at[c, i, 2:4]), at_x
    )
    hn_pair = [copies.make(hng.at[c, i], hng.at[c, i], partner) for i in [x] + xs]

    def hn_first():
        for m in hn_sends:
            m.start()
        hng[c, x, y] = hns[c, y]

    def hn_second():
        for m in hn_sends:
            m.wait_recv()
        hn_ring.start()
        hn_pair[0].start()

    def hn_third():
        hn_ring.middle()
        hn_pair[1].start()
        hn_pair[2].start()

    def hn_fourth():
        hn_ring.end()
        hn_pair[3].start()

    def partial_output(q, left, w):
        def body(i, carry):
            for j in range(2):
                total = None
                for h in range(2):
                    part = dot(
                        left[h, 2 * j:2 * j + 2].reshape(256, 256),
                        wg[w, i, 4 * h:4 * h + 4].reshape(256, 256),
                        1, 0,
                    )
                    total = part if total is None else total + part
                rsb[q, i, 2 * j:2 * j + 2] = total.astype(BF).reshape(2, 128, 256)
            return carry

        lax.fori_loop(0, NX, body, 0)

    reduce_a1 = RingReduce(
        copies, x,
        lambda i: rsb.at[:, i, :, 0:64],
        lambda i: (rsb.at[:, i, 0:2, 0:64], rsb.at[:, i, 2:4, 0:64]),
        at_x, (a1u, a1d, a2u, a2d),
    )
    reduce_b1 = RingReduce(
        copies, y,
        lambda j: rsb.at[:, :, j, 64:128],
        lambda j: (rsb.at[:, 0:2, j, 64:128], rsb.at[:, 2:4, j, 64:128]),
        at_y, (b1u, b1d, b2u, b2d),
    )
    reduce_a2 = RingReduce(
        copies, y,
        lambda j: sa.at[:, j],
        lambda j: (sa.at[:, j, 0:32], sa.at[:, j, 32:64]),
        at_y, (a3u, a3d, a4u, a4d),
    )
    reduce_b2 = RingReduce(
        copies, x,
        lambda i: sb.at[:, i],
        lambda i: (sb.at[:, i, 0:32], sb.at[:, i, 32:64]),
        at_x, (b3u, b3d, b4u, b4d),
    )
    def outputs():
        partial_output(0, an, 1)
        partial_output(1, hg, 0)
        reduce_a1.start()
        reduce_b1.start()

    def reduce_second():
        reduce_a1.middle()
        reduce_b1.middle()

    def reduce_third():
        sa[...] = reduce_a1.end().astype(BF)
        reduce_a2.start()
        sb[...] = reduce_b1.end().astype(BF)
        reduce_b2.start()

    def reduce_fourth():
        reduce_a2.middle()
        reduce_b2.middle()

    def reduce_last():
        for rows, ring in ((slice(0, 64), reduce_a2), (slice(64, 128), reduce_b2)):
            total = ring.end()
            out[rows, :] = total[0].astype(BF)
            ig[rows, :] = total[1].astype(BF)

    at(29.9, "hidden", hidden_sums)
    at(32.0, "hidden_grad", hidden_gradient)
    at(33.4, "hidden_acts", hidden_acts)
    at(33.6, "hn1", hn_first)
    at(33.8, "grad0", lambda: partial_gradient(0, hgt, 2))
    at(35.1, "outputs", outputs)
    for time, name, act in zip(
        LATE, ("hn2", "rs2", "hn3", "rs3", "hn4", "rs4", "rs5"),
        (hn_second, reduce_second, hn_third, reduce_third, hn_fourth, reduce_fourth, reduce_last),
    ):
        at(time, name, act)

    for time, _, name, act in sorted(steps, key=lambda step: step[:2]):
        with jax.named_scope(f"line_{name}"):
            line_until(time)
        with jax.named_scope(name):
            act()
    with jax.named_scope("line_rest"):
        line_until(1e9)

    def line_end(w):
        for plane in range(NZ):

            @pl.when(z == plane)
            def _():
                for way, buf, outer in ((0, rr, 0), (1, rl, NZ - 1)):
                    if plane == outer:
                        buf[w, plane] = jnp.zeros((4, 64, 256), BF)
                    else:
                        for part in range(PARTS):
                            line_copy(plane, way, w, plane, part)[0].wait_recv()

        fg[w] = (
            grd[w, :, z].astype(F32) + rr[w, z].astype(F32) + rl[w, z].astype(F32)
        ).astype(BF)
        final = [copies.make(fg.at[w, i], fr.at[w, x], at_x(i)) for i in xs]
        for s in final:
            s.start()
        fr[w, x] = fg[w, x]
        return final

    with jax.named_scope("line_end"):
        final = line_end(1) + line_end(0)
    with jax.named_scope("final_wait"):
        for s in hn_pair + final:
            s.wait_recv()

    for made in copies.always:
        made.wait_send()
    for way in (0, 1):
        for w in (0, 1):
            for k in range(4):
                for s in range(3):
                    gather_z[w, way, s, k].wait_send()

        @pl.when(sends_far[way])
        def _():
            for w in (0, 1):
                for k in range(4):
                    gather_z[w, way, 3, k].wait_send()

    for plane in range(NZ):

        @pl.when(z == plane)
        def _():
            for _, *step in orders[plane]:
                line_copy(plane, *step)[0].wait_send()


def finish(raw_out, raw_ig, hng, fr, upa, dna, out, hn_out, ig, ua, da):
    @pl.when(pl.program_id(0) == 0)
    def _():
        out[...] = raw_out[...]
        ig[...] = raw_ig[...]
        ua[...] = upa[...] + fr[0].reshape(256, 256).astype(F32).T
        da[...] = dna[...] + fr[1].reshape(256, 256).astype(F32)

    low = lax.broadcasted_iota(jnp.int32, (128, 128), 1) < 64
    for m in range(2):
        for j in range(NY):
            one = hng[0, 2 * m, j].astype(F32)
            two = hng[0, 2 * m + 1, j].astype(F32)
            off = 256 * j + 128 * m
            hn_out[:, off:off + 128] = jnp.where(low, one, pltpu.roll(two, 64, axis=1)).astype(BF)
            hn_out[:, off + 1024:off + 1152] = jnp.where(low, pltpu.roll(one, 64, axis=1), two).astype(BF)


def local(inputs_next, inputs_prev, hidden_prev, cotangent, up_weight, down_weight, up_accum, down_accum):
    vmem = pl.BlockSpec(memory_space=pltpu.VMEM)
    shapes = [
        (128, 8192),
        (256, 256),
        (4, 64, 256),
        (3, 4, 4, 128, 256),
        (4, 64, 256),
        (2, 4, 8, 64, 256),
        (4, 128, 256),
        (2, 4, 128, 256),
        (512, 512),
        (2, 2, 4, 128, 256),
        (2, 2, 4, 128, 256),
        (2, 4, 128, 256),
        (2, 4, 128, 256),
        (2, 4, 128, 256),
        (512, 512),
        (2, 4, 4, 128, 256),
        (2, 4, 64, 256),
        (2, 4, 64, 256),
    ]
    for _ in range(2):
        shapes += [(2, 2, 64, 256)] * 2 + [(2, 4, 64, 256)] * 2
        shapes += [(2, 32, 256)] * 2 + [(2, 64, 256)] * 2
    shapes += [
        (2, 4, 8, 64, 256),
        (2, 8, 4, 64, 256),
        (2, 8, 4, 64, 256),
        (2, 4, 64, 256),
    ]
    raw = [(128, 256), (128, 256), (2, 4, 4, 128, 256), (2, 4, 64, 256)]
    results = pl.pallas_call(
        kernel,
        out_shape=tuple(pltpu.VMEM(s, BF) for s in raw),
        in_specs=[pl.BlockSpec(memory_space=pltpu.HBM)] * 6,
        out_specs=(vmem,) * 4,
        scratch_shapes=[pltpu.VMEM(s, BF) for s in shapes]
        + [pltpu.SemaphoreType.DMA((7,)), pltpu.SemaphoreType.DMA((N_SEMS,)), pltpu.SemaphoreType.DMA((N_SEMS,))],
        compiler_params=pltpu.CompilerParams(
            collective_id=0, has_side_effects=True, vmem_limit_bytes=VMEM_MAIN
        ),
    )(inputs_next, inputs_prev, cotangent, hidden_prev, up_weight, down_weight.reshape(4, 64, 256))

    outs = [
        (inputs_next.shape, BF, (128, 256)),
        (hidden_prev.shape, BF, (128, 2048)),
        (inputs_prev.shape, BF, (128, 256)),
        (up_accum.shape, F32, (256, 256)),
        (down_accum.shape, F32, (256, 256)),
    ]
    whole = pl.BlockSpec((128, 256), lambda i: (0, 0))
    square = pl.BlockSpec((256, 256), lambda i: (0, 0))
    return pl.pallas_call(
        finish,
        grid=(4,),
        out_shape=tuple(jax.ShapeDtypeStruct(s, d) for s, d, _ in outs),
        in_specs=[
            whole, whole,
            pl.BlockSpec((1, 4, 4, 128, 128), lambda i: (i // 2, 0, 0, 0, i % 2)),
            pl.BlockSpec((2, 4, 64, 256), lambda i: (0, 0, 0, 0)),
            square, square,
        ],
        out_specs=tuple(
            pl.BlockSpec(b, (lambda i: (0, i)) if n == 1 else (lambda i: (0, 0)))
            for n, (_, _, b) in enumerate(outs)
        ),
        compiler_params=pltpu.CompilerParams(vmem_limit_bytes=16 * 1024 * 1024),
    )(*results, up_accum, down_accum)


def solution(mesh):
    rep_fs, fs = ("rep", "fs"), "fs"
    in_specs = (
        P(rep_fs, "tp"),
        P(rep_fs, "tp"),
        P(rep_fs, None),
        P(rep_fs, "tp"),
        P("tp", fs),
        P(fs, "tp"),
        P(("rep", "tp"), fs),
        P(rep_fs, "tp"),
    )
    out_specs = (
        P(rep_fs, "tp"),
        P(rep_fs, None),
        P(rep_fs, "tp"),
        P(("rep", "tp"), fs),
        P(rep_fs, "tp"),
    )
    return jax.shard_map(local, mesh=mesh, in_specs=in_specs, out_specs=out_specs, check_vma=False)
```

time: 114 us -> 91.6 us (0.80)
  Pallas kernels: 105 us -> 89.2 us
  local copies, waits for them, and re-layouts: 6.68 us -> 0.01 us
    pallas_call x1 -> x2, Pallas kernels: 105 us -> 89.2 us  [the longest x1 86.3 us: local(): pl.pallas_call(kernel, out_shape=tuple((pltpu.VMEM(s, BF) for s in raw)),...]
    unnamed x11 -> x4, local copies, waits for them, and re-layouts: 6.68 us -> 0.01 us
where the time goes in v2:
time: 91.6 us; the launch traced here: 89.9 us
  Pallas kernels  89.2 us (97%)
    pallas_call x1, Pallas kernels, local(): pl.pallas_call(kernel, out_shape=tuple((pltpu.VMEM(s, BF) for s in raw)),...  86.3 us
    pallas_call x1, Pallas kernels, local(): pl.pallas_call(finish, grid=(4,), out_shape=tuple((jax.ShapeDtypeStruct(s...  2.91 us

profile of v2, /device:TPU:1, one launch (start us, length us, event | category | flops | bytes accessed | tf_op | source)
XLA Modules:
  0.0 89.9 jit_solution(1981267328052543250)
XLA Ops:
  0.6 0.0 copy-start.1
  0.6 0.0 copy-start
  0.7 86.3 %shard_map.119 = (bf16[128,256]{1,0:T(8,128)(2,1)S(1)}, bf16[128,256]{1,0:T(8,128)(2,1)S(1)}, bf16[2,4,4,128,256]{4,3,2,1,0:T(8,128)(2,1)S(1)}, bf16[2,4,64,256]{3,2,1,0:T(8,128)(2,1)S(1)}) custom-call(bf16[128,256]{1,0:T(8,128)(2,1)} %xn_hbm.1, bf16[128,256]{1,0:T(8,128)(2,1)} %xp_hbm.1, bf16[128,256]{1,0:T(8,128)(2,1)} %ct_hbm.1, ...), custom_call_target="tpu_custom_call" | custom-call | tf_op jit(solution)/shard_map/pallas_call | solution.py:626
  87.0 0.0 copy-done.1
  87.0 0.0 copy-done
  87.0 2.9 %shard_map.120 = (bf16[128,256]{1,0:T(8,128)(2,1)}, bf16[128,8192]{1,0:T(8,128)(2,1)}, bf16[128,256]{1,0:T(8,128)(2,1)}, f32[256,256]{1,0:T(8,128)}, f32[256,256]{1,0:T(8,128)}) custom-call(bf16[128,256]{1,0:T(8,128)(2,1)S(1)} %get-tuple-element.9.raw_out, bf16[128,256]{1,0:T(8,128)(2,1)S(1)} %get-tuple-element.10.raw_ig, ...), custom_call_target="tpu_custom_call" | custom-call | tf_op jit(solution)/shard_map/pallas_call | solution.py:647
Async XLA Ops:
  0.6 86.3 %copy-start.1 = (f32[256,256]{1,0:T(8,128)S(1)}, f32[256,256]{1,0:T(8,128)}, u32[]{:S(2)}) copy-start(f32[256,256]{1,0:T(8,128)} %dna.1) | copy-start | bytes 786436
  0.6 86.3 %copy-start = (f32[256,256]{1,0:T(8,128)S(1)}, f32[256,256]{1,0:T(8,128)}, u32[]{:S(2)}) copy-start(f32[256,256]{1,0:T(8,128)} %upa.1) | copy-start | bytes 786436

commit v3 on v2

--- a/solution.py
+++ b/solution.py
@@ -1,3 +1,5 @@
+import math
+
 import jax
 import jax.numpy as jnp
 from jax import lax
@@ -11,10 +13,14 @@
 
 NZ, NY, NX = 8, 4, 4
 PARTS = 2
+LATER = 0.0
+VMEM_MAIN = 60 * 1024 * 1024
+W0_READY, W1_READY, EARLY, HOP, LEAD = 35.05, 22.5, 5, 2.5, 0.7
+LATE = (40.0, 43.0, 48.0, 52.0, 55.0, 56.0, 61.0)
 VMEM_MAIN = 60 * 1024 * 1024
 W0_READY, W1_READY, EARLY = 35.05, 19.5, 5
-LATE = (41.0, 44.5, 51.0, 57.0, 60.0, 62.0, 66.0)
-N_SEMS = 256
+LATE = (40.0, 43.0, 48.0, 52.0, 55.0, 56.0, 61.0)
+N_RECV, N_SEND = 139, 19
 
 
 def dot(a, b, ca, cb):
@@ -27,27 +33,35 @@
 
 class Copies:
     def __init__(self, send, recv):
-        self.send, self.recv, self.count, self.always = send, recv, 0, []
-
-    def slot(self):
-        self.count += 1
-        assert self.count <= N_SEMS
-        return self.count - 1
-
-    def at(self, slot, src, dst, to):
+        self.send, self.recv, self.count, self.groups, self.group = send, recv, 0, [], 0
+
+    def slots(self, n):
+        self.count += n
+        assert self.count <= N_RECV
+        return self.count - n
+
+    def begin(self):
+        self.groups.append(0)
+        self.group = len(self.groups) - 1
+        return self.group
+
+    def at(self, slot, group, src, dst, to):
         return pltpu.make_async_remote_copy(
             src_ref=src,
             dst_ref=dst,
-            send_sem=self.send.at[slot],
+            send_sem=self.send.at[group],
             recv_sem=self.recv.at[slot],
             device_id=to,
             device_id_type=MESH,
         )
 
     def make(self, src, dst, to):
-        made = self.at(self.slot(), src, dst, to)
-        self.always.append(made)
-        return made
+        self.groups[self.group] += math.prod(src.shape)
+        return self.at(self.slots(1), self.group, src, dst, to)
+
+    def wait_sent(self, group, size, ref):
+        part = ref.at[:, 0:size // 128]
+        pltpu.make_async_copy(part, part, self.send.at[group]).wait()
 
 
 class RingGather:
@@ -112,7 +126,7 @@
 def line_order(ready, early):
     orders = [[] for _ in range(NZ)]
     for way in (0, 1):
-        free = [5.0 + 5.6 * n for n in (3, 3, 3, 4, 4, 4, 4)]
+        free = [W1_READY, 26.0, 26.0, 30.0, 30.0, 30.0, 30.0]
         queue = []
         for turn in range(NZ - 1):
             for part in range(PARTS):
@@ -124,18 +138,18 @@
                 plane = hop if way == 0 else NZ - 1 - hop
                 dest = NZ - 1 - turn if way == 0 else turn
                 begin = max(free[hop], at)
-                orders[plane].append((max(at, begin - 0.7) if hop == 0 else at, way, weight, dest, part))
+                orders[plane].append((max(at, begin - LEAD) if hop == 0 else at, way, weight, dest, part))
                 free[hop] = begin + 2.8 / PARTS
-                at = begin + 2.8 / PARTS + 2.5
+                at = begin + 2.8 / PARTS + HOP
     return [sorted(o) for o in orders]
 
 
 def kernel(
     xn_hbm, xp_hbm, ct_hbm, hp_hbm, up_hbm, dn_hbm,
     out, ig, hng, fr,
-    hp, upw, dnw, tok, ut, wg, hps, hpf, apt, hpo, hpi, hns, an, hg, hgt, rsb, sa, sb,
+    hp, upw, own, tok, wg, hps, hpf, apt, hpo, hpi, hns, an, hg, hgt, rsb, sa, sb,
     a1u, a1d, a2u, a2d, a3u, a3d, a4u, a4d, b1u, b1d, b2u, b2d, b3u, b3d, b4u, b4d,
-    grd, rr, rl, fg, load, send, recv,
+    grd, line, fg, sums, load, send, recv,
 ):
     r, f, t = lax.axis_index("rep"), lax.axis_index("fs"), lax.axis_index("tp")
     z, y, x, c = f // NY, lax.rem(f, NY), t // 2, lax.rem(t, 2)
@@ -158,8 +172,8 @@
     loads = [
         pltpu.make_async_copy(source, target, load.at[k])
         for k, (source, target) in enumerate((
-            (up_hbm, upw), (dn_hbm, dnw), (dn_hbm.at[x], wg.at[1, x, z]),
-            (ct_hbm, tok.at[1, x, y]), (xn_hbm, tok.at[0, x, y]), (xp_hbm, tok.at[2, x, y]), (hp_hbm, hp),
+            (up_hbm, upw), (dn_hbm, own.at[1]), (dn_hbm.at[x], wg.at[1, x, z]),
+            (ct_hbm, tok.at[0, x, y]), (xn_hbm, tok.at[1, x, y]), (xp_hbm, tok.at[2, x, y]), (hp_hbm, hp),
         ))
     ]
     for made in loads:
@@ -173,64 +187,68 @@
 
     for made in loads[:3]:
         made.wait()
-    ut[...] = upw[...].astype(F32).T.astype(BF).reshape(4, 64, 256)
-    wg[0, x, z] = ut[x]
-    pl.semaphore_wait(barrier, len(peers))
+    own[0] = upw[...].astype(F32).T.astype(BF).reshape(4, 64, 256)
+    wg[0, x, z] = own[0, x]
+    with jax.named_scope("barrier"):
+        pl.semaphore_wait(barrier, len(peers))
 
     steps = []
 
     def at(time, name, act):
         steps.append((time, len(steps), name, act))
 
-    spread = {}
-    for off, i in ((1, xs[0]), (3, xs[1]), (2, xs[2])):
-        for w, source in ((1, dnw), (0, ut)):
-            spread[w, off] = copies.make(source.at[i], wg.at[w, x, z], at_x(i))
-    for off in (1, 3):
-        for w in (1, 0):
-            spread[w, off].start()
-    at(4.65, "spread2", lambda: [spread[w, 2].start() for w in (1, 0)])
+    copies.begin()
+    spread = {off: copies.make(own.at[:, i], wg.at[:, x, z], at_x(i)) for off, i in ((1, xs[0]), (3, xs[1]), (2, xs[2]))}
+    spread[1].start()
+    spread[3].start()
+    at(4.65, "spread2", lambda: spread[2].start())
     slabs = (x, xs[0], xs[1], xs[2])
     gather_z = {}
-    for w in (1, 0):
-        for way, to in ((0, z_up), (1, z_down)):
-            for s in range(4):
-                piece = lax.rem(z + (NZ - s if way == 0 else s), NZ)
-                for k, i in enumerate(slabs):
-                    slot = copies.slot()
-                    gather_z[w, way, s, k] = copies.at(slot, wg.at[w, i, piece], wg.at[w, i, piece], to)
+    z_group = copies.begin()
+    far_groups = (copies.begin(), copies.begin())
+    for way, to in ((0, z_up), (1, z_down)):
+        for s in range(4):
+            piece = lax.rem(z + (NZ - s if way == 0 else s), NZ)
+            for k, i in enumerate(slabs):
+                place = wg.at[:, i, piece]
+                gather_z[way, s, k] = copies.at(
+                    copies.slots(1), z_group if s < 3 else far_groups[way], place, place, to
+                )
 
     sends_far = (jnp.logical_and(z >= 3, z <= 6), jnp.logical_and(z >= 1, z <= 4))
     takes_far = (z >= 4, z < 4)
 
-    def step_z(s, k):
-        if s == 0:
-            if k:
-                for w in (1, 0):
-                    spread[w, (0, 3, 1, 2)[k]].wait_recv()
-            for w in (1, 0):
-                for way in (0, 1):
-                    gather_z[w, way, 0, k].start()
-            return
-        for way in (0, 1):
-            if s <= 3:
-                for w in (1, 0):
-                    gather_z[w, way, s - 1, k].wait_recv()
-                    if s < 3:
-                        gather_z[w, way, s, k].start()
-                if s == 3:
-
-                    @pl.when(sends_far[way])
-                    def _():
-                        for w in (1, 0):
-                            gather_z[w, way, 3, k].start()
-
+    def begin_z(way, k):
+        gather_z[way, 0, k].start()
+
+    def step_z(s, k, way):
+        if s <= 3:
+            gather_z[way, s - 1, k].wait_recv()
+            if s < 3:
+                gather_z[way, s, k].start()
             else:
-
-                @pl.when(takes_far[way])
-                def _():
-                    for w in (1, 0):
-                        gather_z[w, way, 3, k].wait_recv()
+                pl.when(sends_far[way])(lambda: gather_z[way, 3, k].start())
+        else:
+            pl.when(takes_far[way])(lambda: gather_z[way, 3, k].wait_recv())
+
+    def first_z(k):
+        if k:
+            spread[(0, 3, 1, 2)[k]].wait_recv()
+        begin_z(0, k)
+        begin_z(1, k)
+
+    def behind(s):
+        return jnp.logical_and(big_z >= 1, big_z <= s)
+
+    def prompt_z(s, k):
+        if s <= 3:
+            pl.when(jnp.logical_not(behind(s)))(lambda: step_z(s, k, 0))
+        else:
+            step_z(s, k, 0)
+        step_z(s, k, 1)
+
+    def later_z(s, k):
+        pl.when(behind(s))(lambda: step_z(s, k, 0))
 
     z_times = (
         (3.2, 6.5, 6.6, 9.9), (7.15, 10.5, 11.1, 13.3), (13.7, 15.1, 16.5, 18.0),
@@ -238,41 +256,46 @@
     )
     for s, row in enumerate(z_times):
         for k, time in enumerate(row):
-            at(time, f"z{s}{k}", lambda s=s, k=k: step_z(s, k))
-
+            if s == 0:
+                at(time, f"z{s}{k}", lambda k=k: first_z(k))
+            else:
+                at(time, f"z{s}{k}", lambda s=s, k=k: prompt_z(s, k))
+            if 1 <= s <= 3:
+                at(min(time + LATER, 29.8), f"y{s}{k}", lambda s=s, k=k: later_z(s, k))
     for made in loads[3:6]:
         made.wait()
     token_times = {
-        1: ((4.6, 7.25, 10.35), (10.4, 14.95, 18.2), (3.25, 5.8, 8.0), (8.5, 13.2, 16.4)),
-        0: ((11.3, 13.9, 16.75), (16.8, 21.4, 24.6), (3.9, 6.45, 8.7), (15.0, 19.6, 22.8)),
-        2: ((12.0, 14.6, 17.1), (19.65, 24.5, 27.9), (4.7, 7.2, 9.4), (17.7, 23.1, 26.3)),
+        (0, 1): ((4.6, 7.25, 10.35), (10.4, 14.95, 18.2), (3.25, 5.8, 8.0), (8.5, 13.2, 16.4)),
+        (1, 3): ((11.3, 13.9, 16.75), (16.8, 21.4, 24.6), (3.9, 6.45, 8.7), (15.0, 19.6, 22.8)),
     }
-    for k, times in token_times.items():
+    for (k, end), times in token_times.items():
+        copies.begin()
+        ks = slice(k, end)
         first = (
             RingGather(
                 copies, x,
-                lambda i, k=k: tok.at[k, i, y, 0:64],
-                lambda i, k=k: (tok.at[k, i, y, 0:32], tok.at[k, i, y, 32:64]),
+                lambda i, ks=ks: tok.at[ks, i, y, 0:64],
+                lambda i, ks=ks: (tok.at[ks, i, y, 0:32], tok.at[ks, i, y, 32:64]),
                 at_x,
             ),
             RingGather(
                 copies, y,
-                lambda j, k=k: tok.at[k, x, j, 64:128],
-                lambda j, k=k: (tok.at[k, x, j, 64:96], tok.at[k, x, j, 96:128]),
+                lambda j, ks=ks: tok.at[ks, x, j, 64:128],
+                lambda j, ks=ks: (tok.at[ks, x, j, 64:96], tok.at[ks, x, j, 96:128]),
                 at_y,
             ),
         )
         second = (
             RingGather(
                 copies, y,
-                lambda j, k=k: tok.at[k, :, j, 0:64],
-                lambda j, k=k: (tok.at[k, 0:2, j, 0:64], tok.at[k, 2:4, j, 0:64]),
+                lambda j, ks=ks: tok.at[ks, :, j, 0:64],
+                lambda j, ks=ks: (tok.at[ks, 0:2, j, 0:64], tok.at[ks, 2:4, j, 0:64]),
                 at_y,
             ),
             RingGather(
                 copies, x,
-                lambda i, k=k: tok.at[k, i, :, 64:128],
-                lambda i, k=k: (tok.at[k, i, 0:2, 64:128], tok.at[k, i, 2:4, 64:128]),
+                lambda i, ks=ks: tok.at[ks, i, :, 64:128],
+                lambda i, ks=ks: (tok.at[ks, i, 0:2, 64:128], tok.at[ks, i, 2:4, 64:128]),
                 at_x,
             ),
         )
@@ -281,6 +304,7 @@
             for moment, name in zip(moments, ("start", "middle", "end")):
                 at(moment, f"t{k}{label}{name}", getattr(ring, name))
 
+    copies.begin()
     hp_sends = [copies.make(hps.at[j], hpf.at[c, y], at_y(j)) for j in ys]
     hp_pair = copies.make(hpf.at[c], hpf.at[c], partner)
 
@@ -328,47 +352,66 @@
 
         lax.fori_loop(0, NX, body, 0)
 
-    at(18.25, "grad1", lambda: partial_gradient(1, apt, 1))
-
-    line_slots = {
-        (way, w, part): [copies.slot() for _ in range(NZ)]
-        for way in (0, 1) for w in (0, 1) for part in range(PARTS)
-    }
-    line_bufs = (rr, rl)
+    at(18.25, "grad1", lambda: partial_gradient(1, apt, 0))
+
+    line_base = copies.slots(2 * PARTS * (NZ + 1))
+    line_groups = [copies.begin() for _ in range(NZ)]
     size = NX // PARTS
 
-    def line_copy(plane, way, w, dest, part):
-        buf = line_bufs[way]
-        first = plane == (0 if way == 0 else NZ - 1)
-        span = pl.ds(part * size, size)
-        source = grd.at[w, span, dest] if first else buf.at[w, dest, span]
-        to = (r, f + NY if way == 0 else f - NY, t)
-        return copies.at(line_slots[way, w, part][dest], source, buf.at[w, dest, span], to), first
-
-    def line_step(plane, way, w, dest, part):
-        made, first = line_copy(plane, way, w, dest, part)
-        if not first:
-            made.wait_recv()
-            buf = line_bufs[way]
-            for i in range(part * size, part * size + size):
-                add_into(buf.at[w, dest, i], grd.at[w, i, dest])
+    def line_copy(way, w, dest, part):
+        slot = line_base + (w * PARTS + part) * (NZ + 1) + dest + 1 - way
+        place = line.at[way, w, dest, pl.ds(part * size, size)]
+        return copies.at(slot, line_groups[0] + dest, place, place, (r, f + NY - 2 * NY * way, t))
+
+    def line_item(way, turn):
+        dests = jnp.where(way == 0, NZ - 1 - z, z)
+        early = PARTS * jnp.minimum(EARLY, dests)
+        late = turn - early - PARTS * dests
+        w = jnp.where(jnp.logical_or(turn < early, late >= 0), 1, 0)
+        count = jnp.where(turn < early, turn, jnp.where(late < 0, turn - early, early + late))
+        nth = count // PARTS
+        return w, jnp.where(way == 0, NZ - 1 - nth, nth), lax.rem(count, PARTS)
+
+    orders = line_order((W0_READY, W1_READY), EARLY)
+    of_plane = [
+        sum((step[1] << n) for n, step in enumerate(order)) for order in orders
+    ]
+
+    def for_plane(values):
+        found = values[NZ - 1]
+        for plane in range(NZ - 1):
+            found = jnp.where(z == plane, values[plane], found)
+        return found
+
+    ways = for_plane(of_plane)
+
+    def line_body(n, rights):
+        way = lax.rem(lax.shift_right_logical(ways, n), 2)
+        w, dest, part = line_item(way, jnp.where(way == 0, rights, n - rights))
+        made = line_copy(way, w, dest, part)
+        inner = jnp.where(way == 0, z > 0, z < NZ - 1)
+
+        @pl.when(inner)
+        def _():
+            with jax.named_scope("lw"):
+                made.wait_recv()
+
+        for i in range(size):
+            place = line.at[way, w, dest, part * size + i]
+            came = jnp.where(inner, place[...].astype(F32), 0.0)
+            place[...] = (came + grd[w, part * size + i, dest].astype(F32)).astype(BF)
         made.start()
-
-    orders = line_order((W0_READY, W1_READY), EARLY)
-    done = [0] * NZ
+        return rights + 1 - way
+
+    line_done = [0, jnp.int32(0), [0] * NZ]
 
     def line_until(time):
-        for plane in range(NZ):
-            todo = []
-            while done[plane] < len(orders[plane]) and orders[plane][done[plane]][0] <= time:
-                todo.append(orders[plane][done[plane]])
-                done[plane] += 1
-            if todo:
-
-                @pl.when(z == plane)
-                def _():
-                    for _, *step in todo:
-                        line_step(plane, *step)
+        ends = [sum(step[0] <= time for step in order) for order in orders]
+        if ends == line_done[2]:
+            return
+        end = for_plane(ends)
+        line_done[1] = lax.fori_loop(line_done[0], end, line_body, line_done[1])
+        line_done[0], line_done[2] = end, ends
 
     def partial_hidden(q, w):
         def body(j, carry):
@@ -376,7 +419,7 @@
                 total = None
                 for i in range(NX):
                     part = dot(
-                        tok[q, i, pl.ds(2 * j, 2)].reshape(256, 256),
+                        tok[1 - q, i, pl.ds(2 * j, 2)].reshape(256, 256),
                         wg[w, i, 4 * h:4 * h + 4].reshape(256, 256),
                         1, 1,
                     )
@@ -386,6 +429,7 @@
 
         lax.fori_loop(0, 2, body, 0)
 
+    copies.begin()
     pair = [copies.make(hpo.at[q], hpi.at[q], partner) for q in range(2)]
 
     def hidden_sums():
@@ -412,18 +456,22 @@
                 v = relu(hidden.astype(F32))
                 an[h, j] = (v * v).astype(BF)
 
+    copies.begin()
     hn_sends = [copies.make(hns.at[c, j], hng.at[c, x, y], at_y(j)) for j in ys]
     hn_ring = RingGather(
         copies, x, lambda i: hng.at[c, i], lambda i: (hng.at[c, i, 0:2], hng.at[c, i, 2:4]), at_x
     )
     hn_pair = [copies.make(hng.at[c, i], hng.at[c, i], partner) for i in [x] + xs]
 
+    hn_own = pltpu.make_async_copy(hns.at[c, y], hng.at[c, x, y], load.at[7])
+
     def hn_first():
         for m in hn_sends:
             m.start()
-        hng[c, x, y] = hns[c, y]
+        hn_own.start()
 
     def hn_second():
+        hn_own.wait()
         for m in hn_sends:
             m.wait_recv()
         hn_ring.start()
@@ -454,6 +502,7 @@
 
         lax.fori_loop(0, NX, body, 0)
 
+    copies.begin()
     reduce_a1 = RingReduce(
         copies, x,
         lambda i: rsb.at[:, i, :, 0:64],
@@ -498,11 +547,17 @@
         reduce_a2.middle()
         reduce_b2.middle()
 
+    results = [
+        pltpu.make_async_copy(sums.at[k], ref, load.at[8 + k]) for k, ref in enumerate((out, ig))
+    ]
+
     def reduce_last():
         for rows, ring in ((slice(0, 64), reduce_a2), (slice(64, 128), reduce_b2)):
             total = ring.end()
-            out[rows, :] = total[0].astype(BF)
-            ig[rows, :] = total[1].astype(BF)
+            sums[0, rows, :] = total[0].astype(BF)
+            sums[1, rows, :] = total[1].astype(BF)
+        for made in results:
+            made.start()
 
     at(29.9, "hidden", hidden_sums)
     at(32.0, "hidden_grad", hidden_gradient)
@@ -525,52 +580,48 @@
         line_until(1e9)
 
     def line_end(w):
-        for plane in range(NZ):
-
-            @pl.when(z == plane)
+        for way, inner in ((0, z > 0), (1, z < NZ - 1)):
+
+            @pl.when(inner)
             def _():
-                for way, buf, outer in ((0, rr, 0), (1, rl, NZ - 1)):
-                    if plane == outer:
-                        buf[w, plane] = jnp.zeros((4, 64, 256), BF)
-                    else:
-                        for part in range(PARTS):
-                            line_copy(plane, way, w, plane, part)[0].wait_recv()
+                for part in range(PARTS):
+                    line_copy(way, w, z, part).wait_recv()
 
         fg[w] = (
-            grd[w, :, z].astype(F32) + rr[w, z].astype(F32) + rl[w, z].astype(F32)
+            grd[w, :, z].astype(F32)
+            + jnp.where(z > 0, line[0, w, z].astype(F32), 0.0)
+            + jnp.where(z < NZ - 1, line[1, w, z].astype(F32), 0.0)
         ).astype(BF)
-        final = [copies.make(fg.at[w, i], fr.at[w, x], at_x(i)) for i in xs]
-        for s in final:
-            s.start()
-        fr[w, x] = fg[w, x]
-        return final
 
     with jax.named_scope("line_end"):
-        final = line_end(1) + line_end(0)
+        line_end(1)
+        line_end(0)
+    copies.begin()
+    final = [copies.make(fg.at[:, i], fr.at[:, x], at_x(i)) for i in xs]
+    kept = pltpu.make_async_copy(fg.at[:, x], fr.at[:, x], load.at[10])
+    for s in final + [kept]:
+        s.start()
+    results.append(kept)
     with jax.named_scope("final_wait"):
         for s in hn_pair + final:
             s.wait_recv()
-
-    for made in copies.always:
-        made.wait_send()
-    for way in (0, 1):
-        for w in (0, 1):
-            for k in range(4):
-                for s in range(3):
-                    gather_z[w, way, s, k].wait_send()
-
-        @pl.when(sends_far[way])
-        def _():
-            for w in (0, 1):
-                for k in range(4):
-                    gather_z[w, way, 3, k].wait_send()
-
-    for plane in range(NZ):
-
-        @pl.when(z == plane)
-        def _():
-            for _, *step in orders[plane]:
-                line_copy(plane, *step)[0].wait_send()
+        for s in results:
+            s.wait()
+
+    with jax.named_scope("sent"):
+        for group, total in enumerate(copies.groups):
+            if total:
+                copies.wait_sent(group, total, hp)
+        copies.wait_sent(z_group, 3 * 2 * 4 * 2 * 64 * 256, hp)
+        for way in (0, 1):
+            pl.when(sends_far[way])(lambda: copies.wait_sent(far_groups[way], 4 * 2 * 64 * 256, hp))
+
+        def line_sent(dest, carry):
+            pl.when(dest != z)(lambda: copies.wait_sent(line_groups[0] + dest, 2 * NX * 64 * 256, hp))
+            return carry
+
+        lax.fori_loop(0, NZ, line_sent, 0)
+    assert len(copies.groups) <= N_SEND
 
 
 def finish(raw_out, raw_ig, hng, fr, upa, dna, out, hn_out, ig, ua, da):
@@ -596,9 +647,8 @@
     shapes = [
         (128, 8192),
         (256, 256),
-        (4, 64, 256),
+        (2, 4, 64, 256),
         (3, 4, 4, 128, 256),
-        (4, 64, 256),
         (2, 4, 8, 64, 256),
         (4, 128, 256),
         (2, 4, 128, 256),
@@ -618,18 +668,18 @@
         shapes += [(2, 32, 256)] * 2 + [(2, 64, 256)] * 2
     shapes += [
         (2, 4, 8, 64, 256),
-        (2, 8, 4, 64, 256),
-        (2, 8, 4, 64, 256),
+        (2, 2, 8, 4, 64, 256),
         (2, 4, 64, 256),
+        (2, 128, 256),
     ]
     raw = [(128, 256), (128, 256), (2, 4, 4, 128, 256), (2, 4, 64, 256)]
     results = pl.pallas_call(
         kernel,
         out_shape=tuple(pltpu.VMEM(s, BF) for s in raw),
         in_specs=[pl.BlockSpec(memory_space=pltpu.HBM)] * 6,
-        out_specs=(vmem,) * 4,
+        out_specs=(pl.BlockSpec(memory_space=pl.ANY),) * 4,
         scratch_shapes=[pltpu.VMEM(s, BF) for s in shapes]
-        + [pltpu.SemaphoreType.DMA((7,)), pltpu.SemaphoreType.DMA((N_SEMS,)), pltpu.SemaphoreType.DMA((N_SEMS,))],
+        + [pltpu.SemaphoreType.DMA((11,)), pltpu.SemaphoreType.DMA((N_SEND,)), pltpu.SemaphoreType.DMA((N_RECV,))],
         compiler_params=pltpu.CompilerParams(
             collective_id=0, has_side_effects=True, vmem_limit_bytes=VMEM_MAIN
         ),

time: 91.6 us -> 87.2 us (0.952); the launches traced: 89.9 us -> 87.1 us
  Pallas kernels: 89.2 us -> 86.4 us
    pallas_call x1, Pallas kernels: 86.3 us -> 83.5 us  [local(): pl.pallas_call(kernel, out_shape=tuple((pltpu.VMEM(s, BF) for s in raw)),...]
where the time goes in v3:
time: 87.2 us; the launch traced here: 87.1 us
  Pallas kernels  86.4 us (99%)
    pallas_call x1, Pallas kernels, local(): pl.pallas_call(kernel, out_shape=tuple((pltpu.VMEM(s, BF) for s in raw)),...  83.5 us
    pallas_call x1, Pallas kernels, local(): pl.pallas_call(finish, grid=(4,), out_shape=tuple((jax.ShapeDtypeStruct(s...  2.91 us

profile of v3, /device:TPU:1, one launch (start us, length us, event | category | flops | bytes accessed | tf_op | source)
XLA Modules:
  0.0 87.1 jit_solution(12513129275921648528)
XLA Ops:
  0.6 0.0 copy-start.1
  0.6 0.0 copy-start
  0.7 83.5 %shard_map.119 = (bf16[128,256]{1,0:T(8,128)(2,1)S(1)}, bf16[128,256]{1,0:T(8,128)(2,1)S(1)}, bf16[2,4,4,128,256]{4,3,2,1,0:T(8,128)(2,1)S(1)}, bf16[2,4,64,256]{3,2,1,0:T(8,128)(2,1)S(1)}) custom-call(bf16[128,256]{1,0:T(8,128)(2,1)} %xn_hbm.1, bf16[128,256]{1,0:T(8,128)(2,1)} %xp_hbm.1, bf16[128,256]{1,0:T(8,128)(2,1)} %ct_hbm.1, ...), custom_call_target="tpu_custom_call" | custom-call | tf_op jit(solution)/shard_map/pallas_call | solution.py:676
  84.2 0.0 copy-done.1
  84.2 0.0 copy-done
  84.2 2.9 %shard_map.120 = (bf16[128,256]{1,0:T(8,128)(2,1)}, bf16[128,8192]{1,0:T(8,128)(2,1)}, bf16[128,256]{1,0:T(8,128)(2,1)}, f32[256,256]{1,0:T(8,128)}, f32[256,256]{1,0:T(8,128)}) custom-call(bf16[128,256]{1,0:T(8,128)(2,1)S(1)} %get-tuple-element.9.raw_out, bf16[128,256]{1,0:T(8,128)(2,1)S(1)} %get-tuple-element.10.raw_ig, ...), custom_call_target="tpu_custom_call" | custom-call | tf_op jit(solution)/shard_map/pallas_call | solution.py:697
Async XLA Ops:
  0.6 83.5 %copy-start.1 = (f32[256,256]{1,0:T(8,128)S(1)}, f32[256,256]{1,0:T(8,128)}, u32[]{:S(2)}) copy-start(f32[256,256]{1,0:T(8,128)} %dna.1) | copy-start | bytes 786436
  0.6 83.5 %copy-start = (f32[256,256]{1,0:T(8,128)S(1)}, f32[256,256]{1,0:T(8,128)}, u32[]{:S(2)}) copy-start(f32[256,256]{1,0:T(8,128)} %upa.1) | copy-start | bytes 786436

commit v4 on v3

--- a/solution.py
+++ b/solution.py
@@ -20,7 +20,7 @@
 VMEM_MAIN = 60 * 1024 * 1024
 W0_READY, W1_READY, EARLY = 35.05, 19.5, 5
 LATE = (40.0, 43.0, 48.0, 52.0, 55.0, 56.0, 61.0)
-N_RECV, N_SEND = 139, 19
+N_RECV, N_SEND = 142, 19
 
 
 def dot(a, b, ca, cb):
@@ -383,10 +383,10 @@
             found = jnp.where(z == plane, values[plane], found)
         return found
 
-    ways = for_plane(of_plane)
+    ways = [for_plane([bits >> low & (1 << 28) - 1 for bits in of_plane]) for low in (0, 28)]
 
     def line_body(n, rights):
-        way = lax.rem(lax.shift_right_logical(ways, n), 2)
+        way = lax.rem(jnp.where(n < 28, ways[0] >> jnp.minimum(n, 27), ways[1] >> jnp.maximum(n - 28, 0)), 2)
         w, dest, part = line_item(way, jnp.where(way == 0, rights, n - rights))
         made = line_copy(way, w, dest, part)
         inner = jnp.where(way == 0, z > 0, z < NZ - 1)
@@ -593,15 +593,17 @@
             + jnp.where(z < NZ - 1, line[1, w, z].astype(F32), 0.0)
         ).astype(BF)
 
-    with jax.named_scope("line_end"):
-        line_end(1)
-        line_end(0)
     copies.begin()
-    final = [copies.make(fg.at[:, i], fr.at[:, x], at_x(i)) for i in xs]
-    kept = pltpu.make_async_copy(fg.at[:, x], fr.at[:, x], load.at[10])
-    for s in final + [kept]:
-        s.start()
-    results.append(kept)
+    final = []
+    for w in (1, 0):
+        with jax.named_scope("line_end"):
+            line_end(w)
+        made = [copies.make(fg.at[w, i], fr.at[w, x], at_x(i)) for i in xs]
+        kept = pltpu.make_async_copy(fg.at[w, x], fr.at[w, x], load.at[10 + w])
+        for m in made + [kept]:
+            m.start()
+        final += made
+        results.append(kept)
     with jax.named_scope("final_wait"):
         for s in hn_pair + final:
             s.wait_recv()
@@ -625,7 +627,10 @@
 
 
 def finish(raw_out, raw_ig, hng, fr, upa, dna, out, hn_out, ig, ua, da):
-    @pl.when(pl.program_id(0) == 0)
+    step = pl.program_id(0)
+    lanes = pl.ds(pl.multiple_of(lax.rem(step, 2) * 128, 128), 128)
+
+    @pl.when(step == 0)
     def _():
         out[...] = raw_out[...]
         ig[...] = raw_ig[...]
@@ -635,8 +640,8 @@
     low = lax.broadcasted_iota(jnp.int32, (128, 128), 1) < 64
     for m in range(2):
         for j in range(NY):
-            one = hng[0, 2 * m, j].astype(F32)
-            two = hng[0, 2 * m + 1, j].astype(F32)
+            one = hng[step // 2, 2 * m, j, :, lanes].astype(F32)
+            two = hng[step // 2, 2 * m + 1, j, :, lanes].astype(F32)
             off = 256 * j + 128 * m
             hn_out[:, off:off + 128] = jnp.where(low, one, pltpu.roll(two, 64, axis=1)).astype(BF)
             hn_out[:, off + 1024:off + 1152] = jnp.where(low, pltpu.roll(one, 64, axis=1), two).astype(BF)
@@ -679,7 +684,7 @@
         in_specs=[pl.BlockSpec(memory_space=pltpu.HBM)] * 6,
         out_specs=(pl.BlockSpec(memory_space=pl.ANY),) * 4,
         scratch_shapes=[pltpu.VMEM(s, BF) for s in shapes]
-        + [pltpu.SemaphoreType.DMA((11,)), pltpu.SemaphoreType.DMA((N_SEND,)), pltpu.SemaphoreType.DMA((N_RECV,))],
+        + [pltpu.SemaphoreType.DMA((12,)), pltpu.SemaphoreType.DMA((N_SEND,)), pltpu.SemaphoreType.DMA((N_RECV,))],
         compiler_params=pltpu.CompilerParams(
             collective_id=0, has_side_effects=True, vmem_limit_bytes=VMEM_MAIN
         ),
@@ -692,17 +697,13 @@
         (up_accum.shape, F32, (256, 256)),
         (down_accum.shape, F32, (256, 256)),
     ]
-    whole = pl.BlockSpec((128, 256), lambda i: (0, 0))
     square = pl.BlockSpec((256, 256), lambda i: (0, 0))
     return pl.pallas_call(
         finish,
         grid=(4,),
         out_shape=tuple(jax.ShapeDtypeStruct(s, d) for s, d, _ in outs),
         in_specs=[
-            whole, whole,
-            pl.BlockSpec((1, 4, 4, 128, 128), lambda i: (i // 2, 0, 0, 0, i % 2)),
-            pl.BlockSpec((2, 4, 64, 256), lambda i: (0, 0, 0, 0)),
-            square, square,
+            vmem, vmem, vmem, vmem, square, square,
         ],
         out_specs=tuple(
             pl.BlockSpec(b, (lambda i: (0, i)) if n == 1 else (lambda i: (0, 0)))

time: 87.2 us -> 86.2 us (0.989)
  Pallas kernels: 86.4 us -> 85.1 us
    pallas_call x1, Pallas kernels: 83.5 us -> 82.5 us  [local(): pl.pallas_call(kernel, out_shape=tuple((pltpu.VMEM(s, BF) for s in raw)),...]
where the time goes in v4:
time: 86.2 us; the launch traced here: 85.8 us
  Pallas kernels  85.1 us (99%)
    pallas_call x1, Pallas kernels, local(): pl.pallas_call(kernel, out_shape=tuple((pltpu.VMEM(s, BF) for s in raw)),...  82.5 us
    pallas_call x1, Pallas kernels, local(): pl.pallas_call(finish, grid=(4,), out_shape=tuple((jax.ShapeDtypeStruct(s...  2.61 us

profile of v4, /device:TPU:1, one launch (start us, length us, event | category | flops | bytes accessed | tf_op | source)
XLA Modules:
  0.0 85.8 jit_solution(15059650226400013126)
XLA Ops:
  0.6 0.0 copy-start.1
  0.6 0.0 copy-start
  0.7 82.5 %shard_map.119 = (bf16[128,256]{1,0:T(8,128)(2,1)S(1)}, bf16[128,256]{1,0:T(8,128)(2,1)S(1)}, bf16[2,4,4,128,256]{4,3,2,1,0:T(8,128)(2,1)S(1)}, bf16[2,4,64,256]{3,2,1,0:T(8,128)(2,1)S(1)}) custom-call(bf16[128,256]{1,0:T(8,128)(2,1)} %xn_hbm.1, bf16[128,256]{1,0:T(8,128)(2,1)} %xp_hbm.1, bf16[128,256]{1,0:T(8,128)(2,1)} %ct_hbm.1, ...), custom_call_target="tpu_custom_call" | custom-call | tf_op jit(solution)/shard_map/pallas_call | solution.py:681
  83.2 0.0 copy-done.1
  83.2 0.0 copy-done
  83.2 2.6 %shard_map.120 = (bf16[128,256]{1,0:T(8,128)(2,1)}, bf16[128,8192]{1,0:T(8,128)(2,1)}, bf16[128,256]{1,0:T(8,128)(2,1)}, f32[256,256]{1,0:T(8,128)}, f32[256,256]{1,0:T(8,128)}) custom-call(bf16[128,256]{1,0:T(8,128)(2,1)S(1)} %get-tuple-element.9.raw_out, bf16[128,256]{1,0:T(8,128)(2,1)S(1)} %get-tuple-element.10.raw_ig, ...), custom_call_target="tpu_custom_call" | custom-call | tf_op jit(solution)/shard_map/pallas_call | solution.py:701
Async XLA Ops:
  0.6 82.5 %copy-start.1 = (f32[256,256]{1,0:T(8,128)S(1)}, f32[256,256]{1,0:T(8,128)}, u32[]{:S(2)}) copy-start(f32[256,256]{1,0:T(8,128)} %dna.1) | copy-start | bytes 786436
  0.6 82.5 %copy-start = (f32[256,256]{1,0:T(8,128)S(1)}, f32[256,256]{1,0:T(8,128)}, u32[]{:S(2)}) copy-start(f32[256,256]{1,0:T(8,128)} %upa.1) | copy-start | bytes 786436

commit v5 on v4

--- a/solution.py
+++ b/solution.py
@@ -600,7 +600,7 @@
             line_end(w)
         made = [copies.make(fg.at[w, i], fr.at[w, x], at_x(i)) for i in xs]
         kept = pltpu.make_async_copy(fg.at[w, x], fr.at[w, x], load.at[10 + w])
-        for m in made + [kept]:
+        for m in made[::-1] + [kept]:
             m.start()
         final += made
         results.append(kept)

time: 86.2 us -> 86.1 us (level)
  no operation moved by 1% of the time
where the time goes in v5:
time: 86.1 us; the launch traced here: 85.7 us
  Pallas kernels  85 us (99%)
    pallas_call x1, Pallas kernels, local(): pl.pallas_call(kernel, out_shape=tuple((pltpu.VMEM(s, BF) for s in raw)),...  82.4 us
    pallas_call x1, Pallas kernels, local(): pl.pallas_call(finish, grid=(4,), out_shape=tuple((jax.ShapeDtypeStruct(s...  2.61 us

profile of v5, /device:TPU:1, one launch (start us, length us, event | category | flops | bytes accessed | tf_op | source)
XLA Modules:
  0.0 85.7 jit_solution(1410791835051885722)
XLA Ops:
  0.6 0.0 copy-start.1
  0.6 0.0 copy-start
  0.7 82.4 %shard_map.119 = (bf16[128,256]{1,0:T(8,128)(2,1)S(1)}, bf16[128,256]{1,0:T(8,128)(2,1)S(1)}, bf16[2,4,4,128,256]{4,3,2,1,0:T(8,128)(2,1)S(1)}, bf16[2,4,64,256]{3,2,1,0:T(8,128)(2,1)S(1)}) custom-call(bf16[128,256]{1,0:T(8,128)(2,1)} %xn_hbm.1, bf16[128,256]{1,0:T(8,128)(2,1)} %xp_hbm.1, bf16[128,256]{1,0:T(8,128)(2,1)} %ct_hbm.1, ...), custom_call_target="tpu_custom_call" | custom-call | tf_op jit(solution)/shard_map/pallas_call | solution.py:681
  83.0 0.0 copy-done.1
  83.0 0.0 copy-done
  83.1 2.6 %shard_map.120 = (bf16[128,256]{1,0:T(8,128)(2,1)}, bf16[128,8192]{1,0:T(8,128)(2,1)}, bf16[128,256]{1,0:T(8,128)(2,1)}, f32[256,256]{1,0:T(8,128)}, f32[256,256]{1,0:T(8,128)}) custom-call(bf16[128,256]{1,0:T(8,128)(2,1)S(1)} %get-tuple-element.9.raw_out, bf16[128,256]{1,0:T(8,128)(2,1)S(1)} %get-tuple-element.10.raw_ig, ...), custom_call_target="tpu_custom_call" | custom-call | tf_op jit(solution)/shard_map/pallas_call | solution.py:701
Async XLA Ops:
  0.6 82.4 %copy-start.1 = (f32[256,256]{1,0:T(8,128)S(1)}, f32[256,256]{1,0:T(8,128)}, u32[]{:S(2)}) copy-start(f32[256,256]{1,0:T(8,128)} %dna.1) | copy-start | bytes 786436
  0.6 82.4 %copy-start = (f32[256,256]{1,0:T(8,128)S(1)}, f32[256,256]{1,0:T(8,128)}, u32[]{:S(2)}) copy-start(f32[256,256]{1,0:T(8,128)} %upa.1) | copy-start | bytes 786436
